TPU v7x, 256 devices: a whole 4x4x8 slice. The times are simulated.
256 devices in a mesh: rep: 2 (over z_hi), fs: 16 (over z_lo, y), tp: 8 (over x, core).
Axes of the slice: x: 4, y: 4, z: 8 (z_hi: 2, z_lo: 4; z = z_hi * 4 + z_lo), core: 2. Of those that a mesh axis runs over, the one named last changes fastest.
Arguments:
- activations: bfloat16 [12288, 2048], P(('rep', 'fs'), 'tp'), may hold values from -16 to 16
- norm_gain: float32 [2048], replicated, may hold values from 0.1 to 1.9
- query_weight: bfloat16 [2048, 512], P('fs', 'tp'), may hold values from -0.125 to 0.125
- key_weight: bfloat16 [2048, 512], P('fs', 'tp'), may hold values from -0.125 to 0.125
- value_weight: bfloat16 [2048, 512], P('fs', 'tp'), may hold values from -0.125 to 0.125
- gate_weight: bfloat16 [2048, 512], P('fs', 'tp'), may hold values from -0.125 to 0.125
- out_weight: bfloat16 [512, 2048], P('tp', 'fs'), may hold values from -0.25 to 0.25
- mlp_gain: float32 [2048], replicated, may hold values from 0.1 to 1.9
- up_weight: bfloat16 [2048, 8192], P('fs', 'tp'), may hold values from -0.125 to 0.125
- down_weight: bfloat16 [8192, 2048], P('tp', 'fs'), may hold values from -0.0625 to 0.0625
Outputs:
- layer_out: bfloat16 [12288, 2048], P(('rep', 'fs'), 'tp')
All inputs are finite; a program needn't handle non-finite values.
Results may differ from a plain program's by a relative error of at most 0.012.
Values may be sent and summed in bfloat16 or wider, within the bound.
A program may use at most 64 MiB of HBM per device.

v0:
```python
import jax
import jax.numpy as jnp
from jax import lax
from jax.sharding import PartitionSpec as P

HEADS = 8
HEAD_DIM = 64
BLOCK = 64
SEQ_LEN = 128


EPSILON = 1e-06


def rows_first(arrays, axis, dims):
    turned = [jnp.moveaxis(a, dim, 0) for a, dim in zip(arrays, dims)]
    widths = [t[0].size for t in turned]
    both = jnp.concatenate([t.reshape(-1, w) for t, w in zip(turned, widths)], axis=1)
    whole = lax.all_gather(both, axis, axis=0, tiled=True)
    pieces = jnp.split(whole, [sum(widths[:k]) for k in range(1, len(widths))], axis=1)
    return tuple(
        (
            jnp.moveaxis(b.reshape(-1, *t.shape[1:]), 0, dim)
            for b, t, dim in zip(pieces, turned, dims)
        )
    )


def joined_along(pieces, dim):
    pieces = jnp.moveaxis(pieces, 0, dim)
    lengths = pieces.shape
    return pieces.reshape(*lengths[:dim], lengths[dim] * lengths[dim + 1], *lengths[dim + 2 :])


def from_everyone(x, axis):
    copies = jnp.broadcast_to(x, (lax.axis_size(axis), *x.shape))
    return lax.all_to_all(copies, axis, split_axis=0, concat_axis=0, tiled=True)


def gathered_copies(x, axis, dim):
    return joined_along(from_everyone(x, axis), dim)


def sent_together(arrays, axis, dim, along):
    both = jnp.concatenate(arrays, axis=along)
    whole, at, done = (lax.all_gather(both, axis, axis=dim, tiled=True), 0, [])
    for a in arrays:
        done.append(lax.slice_in_dim(whole, at, at + a.shape[along], axis=along))
        at += a.shape[along]
    return tuple(done)


def cut_along(x, dim, devices):
    before, after = (x.shape[:dim], x.shape[dim + 1 :])
    return jnp.moveaxis(x.reshape(*before, devices, -1, *after), dim, 0)


def sum_at_owner(x, axis, dim):
    devices = lax.axis_size(axis)
    pieces = lax.all_to_all(cut_along(x, dim, devices), axis, 0, 0, tiled=True)
    return jnp.sum(pieces.astype(jnp.float32), axis=0)


def rms_norm(rows, gain):
    floats = rows.astype(jnp.float32)
    scaled = floats * lax.rsqrt(jnp.mean(floats * floats, axis=-1, keepdims=True) + EPSILON)
    return (scaled * gain).astype(jnp.bfloat16)


def rotate(raw, cosine, sine, seqs, heads):
    half = HEAD_DIM // 2
    shaped = raw.reshape(seqs, SEQ_LEN, heads, HEAD_DIM)
    first, second = (shaped[..., :half], shaped[..., half:])
    return jnp.concatenate(
        [first * cosine - second * sine, second * cosine + first * sine], axis=-1
    )


def retain(query_raw, key_raw, value_rows, gate_rows, first_head):
    tokens = query_raw.shape[0]
    heads = query_raw.shape[1] // HEAD_DIM
    seqs = tokens // SEQ_LEN
    blocks = SEQ_LEN // BLOCK
    half = HEAD_DIM // 2
    position = jnp.arange(SEQ_LEN, dtype=jnp.float32)
    freqs = 10000.0 ** (-jnp.arange(half, dtype=jnp.float32) / half)
    angle = position[:, None] * freqs[None, :]
    cosine = jnp.cos(angle)[:, None, :]
    sine = jnp.sin(angle)[:, None, :]
    shape_five = (seqs, blocks, BLOCK, heads, HEAD_DIM)
    queries = rotate(query_raw, cosine, sine, seqs, heads).astype(jnp.bfloat16).reshape(shape_five)
    key_block = (
        (rotate(key_raw, cosine, sine, seqs, heads) * HEAD_DIM ** (-0.5))
        .astype(jnp.bfloat16)
        .reshape(shape_five)
    )
    value_block = value_rows.reshape(shape_five)
    head_index = first_head + jnp.arange(heads, dtype=jnp.float32)
    exponent = 5.0 + 4.0 * head_index / (HEADS - 1)
    log_gamma = jnp.log(1.0 - jnp.power(2.0, -exponent))
    offsets = jnp.arange(BLOCK, dtype=jnp.float32)
    distance = offsets[:, None] - offsets[None, :]
    decay_mask = jnp.where(
        distance[None] >= 0,
        jnp.exp(jnp.maximum(distance, 0.0)[None] * log_gamma[:, None, None]),
        0.0,
    )
    scores = jnp.einsum(
        "snbhd,snchd->snhbc", queries, key_block, preferred_element_type=jnp.float32
    )
    weights = (scores * decay_mask[None, None]).astype(jnp.bfloat16)
    inner = jnp.einsum(
        "snhbc,snchd->snbhd", weights, value_block, preferred_element_type=jnp.float32
    )
    query_decay = (
        queries.astype(jnp.float32)
        * jnp.exp((offsets + 1.0)[:, None] * log_gamma[None, :])[:, :, None]
    )
    key_decay = (
        key_block.astype(jnp.float32)
        * jnp.exp((BLOCK - 1.0 - offsets)[:, None] * log_gamma[None, :])[:, :, None]
    )
    block_decay = jnp.exp(BLOCK * log_gamma)[None, :, None, None]

    def advance(state, inputs):
        query_now, key_now, value_now = inputs
        carried = jnp.einsum("sbhd,shde->sbhe", query_now, state)
        state = state * block_decay + jnp.einsum("sbhd,sbhe->shde", key_now, value_now)
        return (state, carried)

    initial = jnp.zeros((seqs, heads, HEAD_DIM, HEAD_DIM), jnp.float32)
    _, cross = lax.scan(
        advance,
        initial,
        (
            jnp.moveaxis(query_decay, 1, 0),
            jnp.moveaxis(key_decay, 1, 0),
            jnp.moveaxis(value_block.astype(jnp.float32), 1, 0),
        ),
    )
    mixed = (inner + jnp.moveaxis(cross, 0, 1)).reshape(tokens, heads, HEAD_DIM)
    centred = mixed - jnp.mean(mixed, axis=-1, keepdims=True)
    normed = centred * lax.rsqrt(jnp.mean(centred * centred, axis=-1, keepdims=True) + EPSILON)
    gated = normed * jax.nn.silu(gate_rows.reshape(tokens, heads, HEAD_DIM))
    return gated.reshape(tokens, heads * HEAD_DIM).astype(jnp.bfloat16)


def local(
    activations,
    norm_gain,
    query_weight,
    key_weight,
    value_weight,
    gate_weight,
    out_weight,
    mlp_gain,
    up_weight,
    down_weight,
):
    up_whole, down_whole = rows_first((up_weight, down_weight), "fs", (0, 1))
    full_rows = gathered_copies(activations, "tp", 1)
    normed = rms_norm(full_rows, norm_gain)
    head_width = query_weight.shape[1]
    pieces = sent_together((query_weight, key_weight, value_weight, gate_weight), "fs", 0, 1)
    query_raw, key_raw, value_raw, gate_rows = tuple(
        (jnp.dot(normed, piece, preferred_element_type=jnp.float32) for piece in pieces)
    )
    first_head = (lax.axis_index("tp") * (head_width // HEAD_DIM)).astype(jnp.float32)
    retained = retain(query_raw, key_raw, value_raw.astype(jnp.bfloat16), gate_rows, first_head)
    partial_mix = jnp.dot(
        retained, gathered_copies(out_weight, "fs", 1), preferred_element_type=jnp.float32
    )
    branch = sum_at_owner(partial_mix.astype(jnp.bfloat16), "tp", 1)
    middle = (activations.astype(jnp.float32) + branch).astype(jnp.bfloat16)
    middle_rows = gathered_copies(middle, "tp", 1)
    second = rms_norm(middle_rows, mlp_gain)
    hidden = jnp.square(
        jax.nn.relu(jnp.dot(second, up_whole, preferred_element_type=jnp.float32))
    ).astype(jnp.bfloat16)
    down_part = jnp.dot(hidden, down_whole, preferred_element_type=jnp.float32)
    summed = sum_at_owner(down_part.astype(jnp.bfloat16), "tp", 1)
    return (middle.astype(jnp.float32) + summed).astype(jnp.bfloat16)


def solution(mesh):
    in_specs = (
        P(("rep", "fs"), "tp"),
        P(),
        P("fs", "tp"),
        P("fs", "tp"),
        P("fs", "tp"),
        P("fs", "tp"),
        P("tp", "fs"),
        P(),
        P("fs", "tp"),
        P("tp", "fs"),
    )
    out_specs = P(("rep", "fs"), "tp")
    return jax.shard_map(local, mesh=mesh, in_specs=in_specs, out_specs=out_specs, check_vma=False)
```

profile of v0, /device:TPU:2, one launch (start us, length us, event | category | flops | bytes accessed | tf_op | source)
XLA Modules:
  0.0 244.7 jit_solution(14522806187578638049)
XLA Ops:
  6.5 1.4 pad_maximum_fusion.1
  8.0 1.1 copy.63
  9.1 1.8 pad_maximum_fusion
  10.9 2.2 broadcast_in_dim.17
  13.2 5.7 %all-to-all-start = ((bf16[8,384,256]{2,1,0:T(8,128)(2,1)}), bf16[8,384,256]{2,1,0:T(8,128)(2,1)S(1)}, u32[]{:S(2)}, u32[]{:S(2)}) async-start(bf16[8,384,256]{2,1,0:T(8,128)(2,1)} %broadcast_in_dim.17), calls=%async_computation | async-start | bytes 3145728 | tf_op jit(solution)/shard_map/all_to_all | solution.py:37
  20.4 18.6 %all-to-all-done = bf16[8,384,256]{2,1,0:T(8,128)(2,1)S(1)} async-done(((bf16[8,384,256]{2,1,0:T(8,128)(2,1)}), bf16[8,384,256]{2,1,0:T(8,128)(2,1)S(1)}, u32[]{:S(2)}, u32[]{:S(2)}) %all-to-all-start) | async-done | bytes 1572896 | tf_op jit(solution)/shard_map/all_to_all | solution.py:37
  39.8 7.7 %all-to-all-start.1 = ((bf16[16,64,128]{2,1,0:T(8,128)(2,1)}), bf16[16,64,128]{2,1,0:T(8,128)(2,1)S(1)}, u32[]{:S(2)}, u32[]{:S(2)}) async-start(bf16[16,64,128]{2,1,0:T(8,128)(2,1)} %broadcast_in_dim.22), calls=%async_computation.1 | async-start | bytes 524288 | tf_op jit(solution)/shard_map/all_to_all | solution.py:37
  48.4 2.1 convert_bitcast_fusion
  50.6 3.6 %copy.47 = f32[384,8,256]{2,1,0:T(8,128)} copy(f32[384,8,256]{0,2,1:T(8,128)} %convert_bitcast_fusion) | data formatting | bytes 6291456 | tf_op jit(solution)/shard_map/convert_element_type | solution.py:65
  54.2 2.8 %reshape.438 = f32[3,128,2048]{2,1,0:T(8,128)S(1)} reshape(f32[384,8,256]{2,1,0:T(8,128)} %copy.47) | data formatting | bytes 6291456 | tf_op jit(solution)/shard_map/convert_element_type | solution.py:65
  57.1 1.8 multiply_reduce_fusion.1
  58.9 3.1 %fusion.22 = bf16[384,2048]{0,1:T(8,128)(2,1)} fusion(bf16[8,384,256]{1,2,0:T(8,128)(2,1)} %copy-done, f32[2048]{0:T(1024)S(1)} %copy-done.3, f32[384]{0:T(512)S(1)} %get-tuple-element.88), kind=kLoop, calls=%fused_computation.26 | loop fusion | flops 3145728 | bytes 3155456 | tf_op jit(solution)/shard_map/convert_element_type | solution.py:67
  62.0 18.4 %all-gather.3.cloned.1.call-done = bf16[2048,256]{0,1:T(8,128)(2,1)} async-done(((bf16[128,256]{0,1:T(8,128)(2,1)}), bf16[2048,256]{0,1:T(8,128)(2,1)}) %all-gather.3.cloned.1.call-update) | async-done | bytes 1048592 | tf_op jit(solution)/shard_map/all_gather | solution.py:46
  80.4 1.6 convolution_bitcast_fusion.3
  82.0 1.6 convolution_bitcast_fusion.4
  84.6 1.9 convolution_convert_fusion.1
  87.3 2.0 while.13
  89.4 1.4 fusion.73
  91.3 2.0 convolution_convert_fusion
  93.5 24.9 %all_to_all.25 = bf16[8,384,256]{2,1,0:T(8,128)(2,1)S(1)} all-to-all(bf16[8,384,256]{2,1,0:T(8,128)(2,1)S(1)} %bitcast.138), channel_id=1, replica_groups=mesh['rep'=2,'fs'=16,'tp'=8] {'tp'}, dimensions={0} | all-to-all | bytes 3145728 | tf_op jit(solution)/shard_map/all_to_all | solution.py:60
  119.0 24.0 %all_to_all.26 = bf16[8,384,256]{1,2,0:T(8,128)(2,1)S(1)} all-to-all(bf16[8,384,256]{1,2,0:T(8,128)(2,1)S(1)} %broadcast_in_dim.23), channel_id=1, replica_groups=mesh['rep'=2,'fs'=16,'tp'=8] {'tp'}, dimensions={0} | all-to-all | bytes 3145728 | tf_op jit(solution)/shard_map/all_to_all | solution.py:37
  143.9 60.8 %all-gather.5.cloned.1.call-done = bf16[2048,2048]{0,1:T(8,128)(2,1)} async-done(((bf16[128,2048]{0,1:T(8,128)(2,1)}), bf16[2048,2048]{0,1:T(8,128)(2,1)}) %all-gather.5.cloned.1.call-update) | async-done | bytes 8388624 | tf_op jit(solution)/shard_map/all_gather | solution.py:19
  204.7 6.9 %fusion.23 = bf16[384,2048]{1,0:T(8,128)(2,1)S(1)} fusion(bf16[2048,2048]{0,1:T(8,128)(2,1)} %all-gather.5.cloned.1.call-done, bf16[384,2048]{0,1:T(8,128)(2,1)S(1)} %fusion.20), kind=kOutput, calls=%fused_computation.32 | convolution fusion | flops 3223191552 | bytes 11534336 | tf_op jit(solution)/shard_map/dot_general | solution.py:180
  211.8 25.1 %all_to_all.27 = bf16[8,384,256]{2,1,0:T(8,128)(2,1)S(1)} all-to-all(bf16[8,384,256]{2,1,0:T(8,128)(2,1)S(1)} %bitcast.139), channel_id=1, replica_groups=mesh['rep'=2,'fs'=16,'tp'=8] {'tp'}, dimensions={0} | all-to-all | bytes 3145728 | tf_op jit(solution)/shard_map/all_to_all | solution.py:60
  (72 shorter events, 10.1 us)
Async XLA Ops:
  6.5 73.8 %all-gather.3.cloned.1.call-start = ((), (), s32[]{:S(2)}) async-start(), calls=%async_computation.5 | async-start | bytes 1114112 | tf_op jit(solution)/shard_map/all_gather | solution.py:46
  8.0 196.8 %all-gather.5.cloned.1.call-start = ((), (), s32[]{:S(2)}) async-start(), calls=%async_computation.6 | async-start | bytes 8912896 | tf_op jit(solution)/shard_map/all_gather | solution.py:19
  9.1 29.9 %copy-start.6 = (bf16[64,128]{1,0:T(8,128)(2,1)S(1)}, bf16[64,128]{1,0:T(8,128)(2,1)}, u32[]{:S(2)}) copy-start(bf16[64,128]{1,0:T(8,128)(2,1)} %param.18) | copy-start | bytes 49156
  13.2 25.9 %all-to-all-start = ((bf16[8,384,256]{2,1,0:T(8,128)(2,1)}), bf16[8,384,256]{2,1,0:T(8,128)(2,1)S(1)}, u32[]{:S(2)}, u32[]{:S(2)}) async-start(bf16[8,384,256]{2,1,0:T(8,128)(2,1)} %broadcast_in_dim.17), calls=%async_computation | async-start | bytes 3145728 | tf_op jit(solution)/shard_map/all_to_all | solution.py:37
  39.8 51.5 %all-to-all-start.1 = ((bf16[16,64,128]{2,1,0:T(8,128)(2,1)}), bf16[16,64,128]{2,1,0:T(8,128)(2,1)S(1)}, u32[]{:S(2)}, u32[]{:S(2)}) async-start(bf16[16,64,128]{2,1,0:T(8,128)(2,1)} %broadcast_in_dim.22), calls=%async_computation.1 | async-start | bytes 524288 | tf_op jit(solution)/shard_map/all_to_all | solution.py:37
  48.4 2.2 copy-start
  54.2 4.7 %copy-start.3 = (f32[2048]{0:T(1024)S(1)}, f32[2048]{0:T(1024)}, u32[]{:S(2)}) copy-start(f32[2048]{0:T(1024)} %param.13) | copy-start | bytes 24580
  80.3 3.3 %copy-start.4 = (f32[128,32]{0,1:T(8,128)S(1)}, f32[128,32]{0,1:T(8,128)}, u32[]{:S(2)}) copy-start(f32[128,32]{0,1:T(8,128)} %get-tuple-element.89) | copy-start | bytes 49156
  80.4 3.3 %copy-start.5 = (f32[128,32]{0,1:T(8,128)S(1)}, f32[128,32]{0,1:T(8,128)}, u32[]{:S(2)}) copy-start(f32[128,32]{0,1:T(8,128)} %get-tuple-element.90) | copy-start | bytes 49156
  83.6 3.5 %copy-start.8 = (f32[64]{0:T(128)S(1)}, f32[64]{0:T(128)}, u32[]{:S(2)}) copy-start(f32[64]{0:T(128)} %get-tuple-element.93) | copy-start | bytes 772
  86.9 4.4 %copy-start.1 = (bf16[384,2048]{0,1:T(8,128)(2,1)S(1)}, bf16[384,2048]{0,1:T(8,128)(2,1)}, u32[]{:S(2)}) copy-start(bf16[384,2048]{0,1:T(8,128)(2,1)} %fusion.22) | copy-start | bytes 4718596
  93.5 25.2 %copy-start.2 = (bf16[384,256]{1,0:T(8,128)(2,1)S(1)}, bf16[384,256]{1,0:T(8,128)(2,1)}, u32[]{:S(2)}) copy-start(bf16[384,256]{1,0:T(8,128)(2,1)} %param.12) | copy-start | bytes 589828
  118.8 24.6 %copy-start.7 = (f32[2048]{0:T(1024)S(1)}, f32[2048]{0:T(1024)}, u32[]{:S(2)}) copy-start(f32[2048]{0:T(1024)} %param.19) | copy-start | bytes 24580
Sparse Core Ops, SparseCore 0:
  9.0 71.2 all-gather.2
  82.1 122.6 all-gather.4
where the time goes:
time: 247 us; the launch traced here: 245 us
  waiting for transfers between devices  97.8 us (40%)
  blocking collectives  74.1 us (30%)
  matrix products  17.4 us (7%)
  local copies, waits for them, and re-layouts  14.2 us (6%)
  between operations  13.9 us (6%)
  other arithmetic  13.8 us (6%)
  starting transfers between devices  13.5 us (5%)
    all_gather x1, waiting for transfers between devices, rows_first(): whole = lax.all_gather(both, axis, axis=0, tiled=True)  60.8 us
    all_to_all x2, blocking collectives, sum_at_owner(): pieces = lax.all_to_all(cut_along(x, dim, devices), axis, 0, 0, tiled=True)  50.1 us
    all_to_all x1, blocking collectives, from_everyone(): return lax.all_to_all(copies, axis, split_axis=0, concat_axis=0, tiled=True)  24 us
    all_to_all x2, waiting for transfers between devices, from_everyone(): return lax.all_to_all(copies, axis, split_axis=0, concat_axis=0, tiled=True)  18.6 us
    all_gather x1, waiting for transfers between devices, sent_together(): whole, at, done = (lax.all_gather(both, axis, axis=dim, tiled=True), 0, [])  18.4 us
    all_to_all x2, starting transfers between devices, from_everyone(): return lax.all_to_all(copies, axis, split_axis=0, concat_axis=0, tiled=True)  13.4 us
    dot_general x1, matrix products, local(): down_part = jnp.dot(hidden, down_whole, preferred_element_type=jnp.float32)  6.92 us
    convert_element_type x2, local copies, waits for them, and re-layouts, rms_norm(): floats = rows.astype(jnp.float32)  6.47 us
  transfers between devices with their start and end apart: 4, of which 3 were waited for; matrix products, arithmetic and copies ran while one was open for 15% of the time, Pallas kernels for 0%

commit v1 on v0

v1 whole, which is shorter than its diff:
```python
import numpy as np
import jax
import jax.numpy as jnp
from jax import lax
from jax.experimental import pallas as pl
from jax.experimental.pallas import tpu as pltpu
from jax.sharding import PartitionSpec as P

HEADS = 8
HEAD_DIM = 64
SEQ_LEN = 128
EPSILON = 1e-06
ROWS = 384
D = 2048
NX = 4
BF = jnp.bfloat16
F32 = jnp.float32
MESH = pl.DeviceIdType.MESH
ATTN, UP, DOWN = 0, 1, 2


def rotary_tables():
    half = HEAD_DIM // 2
    position = np.arange(SEQ_LEN, dtype=np.float32)
    freqs = np.float32(10000.0) ** (-np.arange(half, dtype=np.float32) / np.float32(half))
    angle = position[:, None] * freqs[None, :].astype(np.float32)
    cosine, sine = np.cos(angle), np.sin(angle)
    scale = np.float32(HEAD_DIM**-0.5)
    c = np.concatenate([cosine, cosine, cosine * scale, cosine * scale], axis=1)
    s = np.concatenate([-sine, sine, -sine * scale, sine * scale], axis=1)
    return c.astype(np.float32), s.astype(np.float32)


def log_gammas():
    head = np.arange(HEADS, dtype=np.float32)
    exponent = np.float32(5.0) + np.float32(4.0) * head / np.float32(HEADS - 1)
    return np.log(1.0 - np.power(2.0, -exponent.astype(np.float64)))


def lanes(shape):
    return lax.broadcasted_iota(jnp.int32, shape, len(shape) - 1)


def layer_kernel(
    act_hbm, ng_hbm, qw_hbm, kw_hbm, vw_hbm, gw_hbm, ow_hbm, mg_hbm, uw_hbm, dw_hbm, cos_hbm, sin_hbm,
    out_ref,
    attn, upb, dnb, xall, wo, ret, wide, mid, hid, pps, ppr, rss, rsr,
    small, gains, tables, qkvg, gat, lhs, acc,
    local_sem, ring_send, ring_recv, x_send, x_recv, p_send, p_recv, r_send, r_recv,
):
    rep, fs, tp = lax.axis_index("rep"), lax.axis_index("fs"), lax.axis_index("tp")
    zl, y = lax.div(fs, 4), lax.rem(fs, 4)
    x, core = lax.div(tp, 2), lax.rem(tp, 2)
    zg = rep * 4 + zl

    def y_device(step):
        return {"fs": zl * 4 + lax.rem(y + step + 4, 4)}

    def z_device(step):
        other = lax.rem(zg + step + 8, 8)
        return {"rep": lax.div(other, 4), "fs": lax.rem(other, 4) * 4 + y}

    def x_index(step, c=core):
        return lax.rem(x + step + 4, 4) * 2 + c

    def x_device(step):
        return {"tp": x_index(step)}

    partner = {"tp": x * 2 + (1 - core)}

    loads = [
        pltpu.make_async_copy(qw_hbm, small.at[0], local_sem.at[0]),
        pltpu.make_async_copy(kw_hbm, small.at[1], local_sem.at[1]),
        pltpu.make_async_copy(vw_hbm, small.at[2], local_sem.at[2]),
        pltpu.make_async_copy(gw_hbm, small.at[3], local_sem.at[3]),
        pltpu.make_async_copy(ow_hbm.at[pl.ds(0, 32)], attn.at[0, zl, y, pl.ds(128, 32)], local_sem.at[4]),
        pltpu.make_async_copy(ow_hbm.at[pl.ds(32, 32)], attn.at[1, zl, y, pl.ds(128, 32)], local_sem.at[5]),
        pltpu.make_async_copy(act_hbm, xall.at[tp], local_sem.at[6]),
        pltpu.make_async_copy(uw_hbm.at[:, pl.ds(0, 512)], upb.at[0, zl, y], local_sem.at[7]),
        pltpu.make_async_copy(uw_hbm.at[:, pl.ds(512, 512)], upb.at[1, zl, y], local_sem.at[8]),
        pltpu.make_async_copy(dw_hbm.at[pl.ds(0, 512)], dnb.at[0, zl, y], local_sem.at[9]),
        pltpu.make_async_copy(dw_hbm.at[pl.ds(512, 512)], dnb.at[1, zl, y], local_sem.at[10]),
        pltpu.make_async_copy(ng_hbm, gains.at[0], local_sem.at[11]),
        pltpu.make_async_copy(mg_hbm, gains.at[1], local_sem.at[12]),
        pltpu.make_async_copy(cos_hbm, tables.at[0], local_sem.at[13]),
        pltpu.make_async_copy(sin_hbm, tables.at[1], local_sem.at[14]),
    ]
    for copy in loads:
        copy.start()

    barrier = pltpu.get_barrier_semaphore()
    peers = [y_device(1), y_device(-1), z_device(1), z_device(-1), x_device(1), x_device(-1), x_device(2), partner]
    for peer in peers:
        pl.semaphore_signal(barrier, inc=1, device_id=peer, device_id_type=MESH)
    for copy in loads:
        copy.wait()
    attn[0, zl, y, 0:128, :] = jnp.concatenate([small[0], small[1]], axis=1)
    attn[1, zl, y, 0:128, :] = jnp.concatenate([small[2], small[3]], axis=1)
    pl.semaphore_wait(barrier, len(peers))

    started = []

    def send(src, dst, send_sem, recv_sem, device):
        copy = pltpu.make_async_remote_copy(
            src_ref=src, dst_ref=dst, send_sem=send_sem, recv_sem=recv_sem, device_id=device, device_id_type=MESH
        )
        copy.start()
        started.append(copy)

    def arrive(region, send_sem, recv_sem, device):
        pltpu.make_async_remote_copy(
            src_ref=region, dst_ref=region, send_sem=send_sem, recv_sem=recv_sem, device_id=device, device_id_type=MESH
        ).wait_recv()

    bufs = (attn, upb, dnb)
    depth = (160, 128, 512)

    def along_y(half, phase):
        return (half + phase) % 2 == 0

    def piece(item, half, phase, step, p):
        buf, cut = bufs[item], depth[item] // 2
        if along_y(half, phase):
            j = lax.rem(y + step + 4, 4)
            if phase == 0:
                return buf.at[half, zl, j, pl.ds(p * cut, cut)]
            return buf.at[half, pl.ds(2 * p, 2), j]
        j = lax.rem(zl + step + 4, 4)
        if phase == 0:
            return buf.at[half, j, y, pl.ds(p * cut, cut)]
        return buf.at[half, j, pl.ds(2 * p, 2)]

    def ring_device(half, phase, step):
        return y_device(step) if along_y(half, phase) else z_device(step)

    def ring_sems(item, half, phase, kind):
        k = ((item * 2 + half) * 2 + phase) * 6 + kind
        return ring_send.at[k], ring_recv.at[k]

    def ring_start(item, phase):
        for p in range(2):
            for half in range(2):
                for d in range(2):
                    q = p if d == 0 else 1 - p
                    ref = piece(item, half, phase, 0, q)
                    send(ref, ref, *ring_sems(item, half, phase, 2 * d + q), ring_device(half, phase, 1 - 2 * d))

    def ring_forward(item, phase):
        for half in range(2):
            for d in range(2):
                to = 1 - 2 * d
                ref = piece(item, half, phase, -to, d)
                arrive(ref, *ring_sems(item, half, phase, 2 * d + d), ring_device(half, phase, to))
                send(ref, ref, *ring_sems(item, half, phase, 4 + d), ring_device(half, phase, to))

    def ring_near(item, phase):
        for half in range(2):
            for d in range(2):
                to = 1 - 2 * d
                ref = piece(item, half, phase, -to, 1 - d)
                arrive(ref, *ring_sems(item, half, phase, 2 * d + 1 - d), ring_device(half, phase, to))

    def ring_far(item, phase):
        for half in range(2):
            for d in range(2):
                ref = piece(item, half, phase, 2, d)
                arrive(ref, *ring_sems(item, half, phase, 4 + d), ring_device(half, phase, 1 - 2 * d))

    def x_piece(which, t, p):
        if which == 0:
            return xall.at[t, pl.ds(p * 192, 192)]
        if which == 1:
            return wo.at[t, p]
        return ret.at[t, pl.ds(p * 96, 96)]

    def x_sems(which, kind):
        k = which * 14 + kind
        return x_send.at[k], x_recv.at[k]

    def hand_over(which, place, p):
        ref = x_piece(which, x_index((0, -1, 1, 2)[place]), p)
        send(ref, ref, *x_sems(which, 6 + 2 * place + p), partner)

    def x_start(which):
        for p in range(2):
            for d in range(2):
                q = p if d == 0 else 1 - p
                dst = x_piece(which, tp, q)
                src = attn.at[q, :, :, pl.ds(128, 32)] if which == 1 else dst
                send(src, dst, *x_sems(which, 2 * d + q), x_device(1 - 2 * d))
        for p in range(2):
            dst = x_piece(which, tp, p)
            src = attn.at[p, :, :, pl.ds(128, 32)] if which == 1 else dst
            send(src, dst, *x_sems(which, 6 + p), partner)

    def x_forward(which):
        for d in range(2):
            to = 1 - 2 * d
            ref = x_piece(which, x_index(-to), d)
            arrive(ref, *x_sems(which, 2 * d + d), x_device(to))
            send(ref, ref, *x_sems(which, 4 + d), x_device(to))
            hand_over(which, 1 + d, d)

    def x_near(which):
        for d in range(2):
            to = 1 - 2 * d
            arrive(x_piece(which, x_index(-to), 1 - d), *x_sems(which, 2 * d + 1 - d), x_device(to))
            hand_over(which, 1 + d, 1 - d)

    def x_far(which):
        for d in range(2):
            arrive(x_piece(which, x_index(2), d), *x_sems(which, 4 + d), x_device(1 - 2 * d))
            hand_over(which, 3, d)

    def x_partner(which):
        for place in range(4):
            t = x_index((0, -1, 1, 2)[place], 1 - core)
            for p in range(2):
                arrive(x_piece(which, t, p), *x_sems(which, 6 + 2 * place + p), partner)

    def norm_rows(source, gain):
        @pl.loop(0, ROWS // 16)
        def _(i):
            rows = pl.ds(pl.multiple_of(i * 16, 16), 16)
            blocks = [source[t, rows, :].astype(F32) for t in range(8)]
            squares = blocks[0] * blocks[0]
            for b in blocks[1:]:
                squares = squares + b * b
            scale = lax.rsqrt(jnp.sum(squares, axis=-1, keepdims=True) * (1.0 / D) + EPSILON)
            for t in range(8):
                columns = slice(256 * t, 256 * t + 256)
                wide[rows, columns] = (blocks[t] * scale * gains[gain, :, columns]).astype(BF)

    ring_start(ATTN, 0)
    x_start(0)
    ring_start(UP, 0)
    ring_forward(ATTN, 0)
    ring_near(ATTN, 0)
    x_forward(0)
    ring_far(ATTN, 0)
    ring_start(ATTN, 1)
    ring_forward(UP, 0)
    x_near(0)
    x_far(0)
    ring_forward(ATTN, 1)
    ring_start(DOWN, 0)
    ring_near(UP, 0)
    ring_far(UP, 0)
    ring_start(UP, 1)
    x_partner(0)
    norm_rows(xall, 0)
    ring_near(ATTN, 1)
    ring_far(ATTN, 1)
    x_start(1)
    ring_forward(DOWN, 0)

    weights = jnp.concatenate([attn[h, :, :, 0:128, :].reshape(D, 128) for h in range(2)], axis=1)
    qkvg[...] = jnp.dot(wide[...], weights, preferred_element_type=F32)
    log_gamma = jnp.float32(0.0)
    for h, value in enumerate(log_gammas()):
        log_gamma = jnp.where(tp == h, jnp.float32(value), log_gamma)
    square = (SEQ_LEN, SEQ_LEN)
    distance = (lax.broadcasted_iota(jnp.int32, square, 0) - lanes(square)).astype(F32)
    decay = jnp.where(distance >= 0, jnp.exp(jnp.maximum(distance, 0.0) * log_gamma), 0.0)
    lane = lanes(square)
    first, low = lax.rem(lane, 64) < 32, lane < 64
    for s in range(3):
        rows = slice(SEQ_LEN * s, SEQ_LEN * (s + 1))
        qk, vg = qkvg[rows, 0:128], qkvg[rows, 128:256]
        other = jnp.where(first, pltpu.roll(qk, 96, 1), pltpu.roll(qk, 32, 1))
        turned = (qk * tables[0] + other * tables[1]).astype(BF).astype(F32)
        queries = jnp.where(low, turned, 0.0).astype(BF)
        keys = pltpu.roll(turned, 64, 1).astype(BF)
        scores = lax.dot_general(queries, keys, (((1,), (1,)), ((), ())), preferred_element_type=F32)
        mixed = jnp.dot((scores * decay).astype(BF), vg.astype(BF), preferred_element_type=F32)
        mixed = jnp.where(low, mixed, 0.0)
        mean = jnp.sum(mixed, axis=-1, keepdims=True) * (1.0 / HEAD_DIM)
        centred = jnp.where(low, mixed - mean, 0.0)
        variance = jnp.sum(centred * centred, axis=-1, keepdims=True) * (1.0 / HEAD_DIM)
        gate = pltpu.roll(vg, 64, 1)
        gat[rows, :] = centred * lax.rsqrt(variance + EPSILON) * (gate / (1.0 + jnp.exp(-gate)))
    low = lanes((192, 128)) < 64
    ret[tp] = jnp.where(low, gat[0:192, :], pltpu.roll(gat[192:384, :], 64, 1)).astype(BF)
    x_start(2)
    for h in range(2):
        wo[tp, h] = attn[h, :, :, 128:160, :]
    x_forward(1)
    x_near(1)
    x_forward(2)
    x_near(2)
    x_far(2)
    ring_forward(UP, 1)
    ring_near(DOWN, 0)
    ring_far(DOWN, 0)
    ring_start(DOWN, 1)
    x_far(1)
    x_partner(2)
    x_partner(1)

    for j in range(4):
        a, b = ret[2 * j].astype(F32), ret[2 * j + 1].astype(F32)
        lhs[0:192, 128 * j : 128 * j + 128] = jnp.where(low, a, pltpu.roll(b, 64, 1)).astype(BF)
        lhs[192:384, 128 * j : 128 * j + 128] = jnp.where(low, pltpu.roll(a, 64, 1), b).astype(BF)

    @pl.loop(0, 8)
    def _(t):
        z0, y0 = lax.div(t, 2), lax.rem(t, 2) * 2
        columns = [wo[:, :, z0, y0 + k].reshape(HEADS * HEAD_DIM, 128) for k in range(2)]
        branch = jnp.dot(lhs[...], jnp.concatenate(columns, axis=1), preferred_element_type=F32)
        mid[t] = (xall[t].astype(F32) + branch).astype(BF)

    norm_rows(mid, 1)
    ring_near(UP, 1)
    ring_far(UP, 1)
    for h in range(2):
        raw = jnp.dot(wide[...], upb[h].reshape(D, 512), preferred_element_type=F32)
        raw = jnp.maximum(raw, 0.0)
        hid[:, 512 * h : 512 * h + 512] = (raw * raw).astype(BF)
    ring_forward(DOWN, 1)
    ring_near(DOWN, 1)
    ring_far(DOWN, 1)

    def part(t):
        z0, y0 = lax.div(t, 2), lax.rem(t, 2) * 2
        total = None
        for h in range(2):
            columns = jnp.concatenate([dnb[h, z0, y0], dnb[h, z0, y0 + 1]], axis=1)
            term = jnp.dot(hid[:, 512 * h : 512 * h + 512], columns, preferred_element_type=F32)
            total = term if total is None else total + term
        return total

    for i in (1, 2, 3, 0):
        pps[i] = part(x_index(i, 1 - core)).astype(BF)
        send(pps.at[i], ppr.at[i], p_send.at[i], p_recv.at[i], partner)
    for i in (1, 2, 3, 0):
        total = part(x_index(i))
        arrive(ppr.at[i], p_send.at[i], p_recv.at[i], partner)
        total = total + ppr[i].astype(F32)
        if i:
            rss[i - 1] = total.astype(BF)
            send(rss.at[i - 1], rsr.at[i - 1], r_send.at[i - 1], r_recv.at[i - 1], x_device(i))
        else:
            acc[...] = mid[tp].astype(F32) + total
    for i in range(3):
        arrive(rsr.at[i], r_send.at[i], r_recv.at[i], x_device(i + 1))
    out_ref[...] = (acc[...] + rsr[0].astype(F32) + rsr[1].astype(F32) + rsr[2].astype(F32)).astype(BF)
    for copy in started:
        copy.wait_send()


def local(activations, norm_gain, qw, kw, vw, gw, ow, mlp_gain, uw, dw):
    cosine, sine = rotary_tables()
    operands = (
        activations, norm_gain.reshape(1, D), qw, kw, vw, gw, ow, mlp_gain.reshape(1, D), uw, dw,
        jnp.asarray(cosine), jnp.asarray(sine),
    )
    dma = pltpu.SemaphoreType.DMA
    return pl.pallas_call(
        layer_kernel,
        out_shape=jax.ShapeDtypeStruct((ROWS, D // 8), BF),
        in_specs=[pl.BlockSpec(memory_space=pltpu.HBM)] * len(operands),
        out_specs=pl.BlockSpec(memory_space=pltpu.VMEM),
        scratch_shapes=[
            pltpu.VMEM((2, 4, 4, 160, 128), BF),
            pltpu.VMEM((2, 4, 4, 128, 512), BF),
            pltpu.VMEM((2, 4, 4, 512, 128), BF),
            pltpu.VMEM((8, ROWS, 256), BF),
            pltpu.VMEM((8, 2, 4, 4, 32, 128), BF),
            pltpu.VMEM((8, 192, 128), BF),
            pltpu.VMEM((ROWS, D), BF),
            pltpu.VMEM((8, ROWS, 256), BF),
            pltpu.VMEM((ROWS, 1024), BF),
            pltpu.VMEM((4, ROWS, 256), BF),
            pltpu.VMEM((4, ROWS, 256), BF),
            pltpu.VMEM((3, ROWS, 256), BF),
            pltpu.VMEM((3, ROWS, 256), BF),
            pltpu.VMEM((4, 128, 64), BF),
            pltpu.VMEM((2, 1, D), F32),
            pltpu.VMEM((2, 128, 128), F32),
            pltpu.VMEM((ROWS, 256), F32),
            pltpu.VMEM((ROWS, 128), F32),
            pltpu.VMEM((ROWS, 512), BF),
            pltpu.VMEM((ROWS, 256), F32),
            dma((15,)), dma((72,)), dma((72,)), dma((42,)), dma((42,)), dma((4,)), dma((4,)), dma((3,)), dma((3,)),
        ],
        compiler_params=pltpu.CompilerParams(
            collective_id=0, has_side_effects=True, vmem_limit_bytes=56 * 1024 * 1024
        ),
        name="layer",
    )(*operands)


def solution(mesh):
    in_specs = (
        P(("rep", "fs"), "tp"), P(), P("fs", "tp"), P("fs", "tp"), P("fs", "tp"), P("fs", "tp"), P("tp", "fs"), P(),
        P("fs", "tp"), P("tp", "fs"),
    )
    return jax.shard_map(local, mesh=mesh, in_specs=in_specs, out_specs=P(("rep", "fs"), "tp"), check_vma=False)
```

time: 247 us -> 82.8 us (0.34)
  waiting for transfers between devices: 97.8 us -> 0 us
  Pallas kernels: 0 us -> 77 us
  blocking collectives: 74.1 us -> 0 us
  matrix products: 17.4 us -> 0 us
  between operations: 13.9 us -> 0.01 us
  other arithmetic: 13.8 us -> 0 us
  starting transfers between devices: 13.5 us -> 0 us
  local copies, waits for them, and re-layouts: 14.2 us -> 5.23 us
    all_gather x2 -> x0, waiting for transfers between devices: 79.2 us -> none  [the longest x1 60.8 us: rows_first(): whole = lax.all_gather(both, axis, axis=0, tiled=True)]
    pallas_call x0 -> x1, Pallas kernels: none -> 77 us  [local(): pl.pallas_call(layer_kernel, out_shape=jax.ShapeDtypeStruct((ROWS, D // 8...]
    all_to_all x3 -> x0, blocking collectives: 74.1 us -> none  [the longest x2 50.1 us: sum_at_owner(): pieces = lax.all_to_all(cut_along(x, dim, devices), axis, 0, 0, tiled=True)]
    all_to_all x2 -> x0, waiting for transfers between devices: 18.6 us -> none  [from_everyone(): return lax.all_to_all(copies, axis, split_axis=0, concat_axis=0, tiled=True)]
    dot_general x10 -> x0, matrix products: 17.4 us -> none  [the longest x1 6.92 us: local(): down_part = jnp.dot(hidden, down_whole, preferred_element_type=jnp.float32)]
    all_to_all x2 -> x0, starting transfers between devices: 13.4 us -> none  [from_everyone(): return lax.all_to_all(copies, axis, split_axis=0, concat_axis=0, tiled=True)]
    convert_element_type x3 -> x0, local copies, waits for them, and re-layouts: 6.63 us -> none  [the longest x2 6.47 us: rms_norm(): floats = rows.astype(jnp.float32)]
    convert_element_type x5 -> x0, other arithmetic: 6.36 us -> none  [the longest x2 3.48 us: rms_norm(): return (scaled * gain).astype(jnp.bfloat16)]
  transfers between devices with their start and end apart: 4 -> 0, of which waited for: 3 -> 0; matrix products, arithmetic and copies ran while one was open for 15% -> 0% of each run, Pallas kernels for 0% -> 0%
where the time goes in v1:
time: 82.8 us; the launch traced here: 82.2 us
  Pallas kernels  77 us (93%)
  local copies, waits for them, and re-layouts  5.23 us (6%)
    pallas_call x1, Pallas kernels, local(): pl.pallas_call(layer_kernel, out_shape=jax.ShapeDtypeStruct((ROWS, D // 8...  77 us
    unnamed x11, local copies, waits for them, and re-layouts  5.23 us

profile of v1, /device:TPU:2, one launch (start us, length us, event | category | flops | bytes accessed | tf_op | source)
XLA Modules:
  0.0 82.2 jit_solution(5018050994377340946)
XLA Ops:
  0.0 0.0 copy-start
  0.0 1.4 %copy.13.qw_hbm = bf16[128,64]{1,0:T(8,128)(2,1)} copy(bf16[128,64]{0,1:T(8,128)(2,1)} %param.14) | data formatting | bytes 32768 | tf_op args[2]
  1.4 0.0 copy-done
  1.5 0.0 copy-start.1
  1.5 0.7 copy.14.kw_hbm
  2.2 0.0 copy-done.1
  2.2 0.0 copy-start.2
  2.2 0.7 copy.15.vw_hbm
  2.9 0.0 copy-done.2
  2.9 0.7 copy.16.gw_hbm
  3.6 77.0 %layer.1 = bf16[384,256]{1,0:T(8,128)(2,1)} custom-call(bf16[384,256]{1,0:T(8,128)(2,1)} %act_hbm.1, f32[1,2048]{1,0:T(1,128)} %bitcast.2, bf16[128,64]{1,0:T(8,128)(2,1)} %copy.13.qw_hbm, bf16[128,64]{1,0:T(8,128)(2,1)} %copy.14.kw_hbm, bf16[128,64]{1,0:T(8,128)(2,1)} %copy.15.vw_hbm, bf16[128,64]{1,0:T(8,128)(2,1)} %copy.16.gw_hbm, ...), custom_call_target="tpu_custom_call" | custom-call | tf_op jit(solution)/shard_map/layer/pallas_call | solution.py:358
  80.6 1.6 %copy.18 = bf16[384,256]{1,0:T(8,128)(2,1)} copy(bf16[384,256]{1,0:T(8,128)(2,1)} %layer.1) | data formatting | bytes 393216
Async XLA Ops:
  0.0 1.5 %copy-start = (bf16[128,64]{0,1:T(8,128)(2,1)S(1)}, bf16[128,64]{0,1:T(8,128)(2,1)}, u32[]{:S(2)}) copy-start(bf16[128,64]{0,1:T(8,128)(2,1)} %param.15) | copy-start | bytes 49156
  1.5 0.7 copy-start.1
  2.2 0.7 copy-start.2

commit v2 on v1

--- a/solution.py
+++ b/solution.py
@@ -17,6 +17,7 @@
 F32 = jnp.float32
 MESH = pl.DeviceIdType.MESH
 ATTN, UP, DOWN = 0, 1, 2
+ORDER = ((0, 1, -1, 2), (-1, 2, 0, 1))
 
 
 def rotary_tables():
@@ -46,7 +47,7 @@
     out_ref,
     attn, upb, dnb, xall, wo, ret, wide, mid, hid, pps, ppr, rss, rsr,
     small, gains, tables, qkvg, gat, lhs, acc,
-    local_sem, ring_send, ring_recv, x_send, x_recv, p_send, p_recv, r_send, r_recv,
+    local_sem, first_send, first_recv, second_send, second_recv, x_send, x_recv, p_send, p_recv, r_send, r_recv,
 ):
     rep, fs, tp = lax.axis_index("rep"), lax.axis_index("fs"), lax.axis_index("tp")
     zl, y = lax.div(fs, 4), lax.rem(fs, 4)
@@ -89,13 +90,14 @@
         copy.start()
 
     barrier = pltpu.get_barrier_semaphore()
-    peers = [y_device(1), y_device(-1), z_device(1), z_device(-1), x_device(1), x_device(-1), x_device(2), partner]
+    peers = [y_device(1), y_device(-1), z_device(1), z_device(-1), partner]
+    peers += [{"tp": x_index(step, c)} for step in (1, -1, 2) for c in range(2)]
     for peer in peers:
         pl.semaphore_signal(barrier, inc=1, device_id=peer, device_id_type=MESH)
     for copy in loads:
         copy.wait()
-    attn[0, zl, y, 0:128, :] = jnp.concatenate([small[0], small[1]], axis=1)
-    attn[1, zl, y, 0:128, :] = jnp.concatenate([small[2], small[3]], axis=1)
+    for h in range(2):
+        attn[h, zl, y, 0:128, :] = small[2 * h : 2 * h + 2].reshape(128, 128).astype(F32).T.astype(BF)
     pl.semaphore_wait(barrier, len(peers))
 
     started = []
@@ -115,56 +117,88 @@
     bufs = (attn, upb, dnb)
     depth = (160, 128, 512)
 
+    def block(item, half, dz, dy):
+        return bufs[item].at[half, lax.rem(zl + dz + 4, 4), lax.rem(y + dy + 4, 4)]
+
     def along_y(half, phase):
         return (half + phase) % 2 == 0
 
-    def piece(item, half, phase, step, p):
-        buf, cut = bufs[item], depth[item] // 2
-        if along_y(half, phase):
-            j = lax.rem(y + step + 4, 4)
-            if phase == 0:
-                return buf.at[half, zl, j, pl.ds(p * cut, cut)]
-            return buf.at[half, pl.ds(2 * p, 2), j]
-        j = lax.rem(zl + step + 4, 4)
-        if phase == 0:
-            return buf.at[half, j, y, pl.ds(p * cut, cut)]
-        return buf.at[half, j, pl.ds(2 * p, 2)]
+    def piece(item, half, step, p):
+        cut = depth[item] // 2
+        dz, dy = (0, step) if half == 0 else (step, 0)
+        return block(item, half, dz, dy).at[pl.ds(p * cut, cut)]
 
     def ring_device(half, phase, step):
         return y_device(step) if along_y(half, phase) else z_device(step)
 
-    def ring_sems(item, half, phase, kind):
-        k = ((item * 2 + half) * 2 + phase) * 6 + kind
-        return ring_send.at[k], ring_recv.at[k]
-
-    def ring_start(item, phase):
-        for p in range(2):
+    def first_sems(item, half, d, kind):
+        k = ((item * 2 + half) * 2 + d) * 3 + kind
+        return first_send.at[k], first_recv.at[k]
+
+    def first_start(item):
+        for n in range(2):
             for half in range(2):
                 for d in range(2):
-                    q = p if d == 0 else 1 - p
-                    ref = piece(item, half, phase, 0, q)
-                    send(ref, ref, *ring_sems(item, half, phase, 2 * d + q), ring_device(half, phase, 1 - 2 * d))
-
-    def ring_forward(item, phase):
+                    p = n if d == 0 else 1 - n
+                    ref = piece(item, half, 0, p)
+                    send(ref, ref, *first_sems(item, half, d, n), ring_device(half, 0, 1 - 2 * d))
+
+    def first_forward(item):
         for half in range(2):
             for d in range(2):
                 to = 1 - 2 * d
-                ref = piece(item, half, phase, -to, d)
-                arrive(ref, *ring_sems(item, half, phase, 2 * d + d), ring_device(half, phase, to))
-                send(ref, ref, *ring_sems(item, half, phase, 4 + d), ring_device(half, phase, to))
-
-    def ring_near(item, phase):
+                ref = piece(item, half, -to, d)
+                arrive(ref, *first_sems(item, half, d, 0), ring_device(half, 0, to))
+                send(ref, ref, *first_sems(item, half, d, 2), ring_device(half, 0, to))
+
+    def first_near(item):
         for half in range(2):
             for d in range(2):
                 to = 1 - 2 * d
-                ref = piece(item, half, phase, -to, 1 - d)
-                arrive(ref, *ring_sems(item, half, phase, 2 * d + 1 - d), ring_device(half, phase, to))
-
-    def ring_far(item, phase):
+                arrive(piece(item, half, -to, 1 - d), *first_sems(item, half, d, 1), ring_device(half, 0, to))
+
+    def first_far(item):
         for half in range(2):
             for d in range(2):
-                ref = piece(item, half, phase, 2, d)
-                arrive(ref, *ring_sems(item, half, phase, 4 + d), ring_device(half, phase, 1 - 2 * d))
+                arrive(piece(item, half, 2, d), *first_sems(item, half, d, 2), ring_device(half, 0, 1 - 2 * d))
+
+    def second_block(item, half, step, d, n):
+        across = ORDER[d][n]
+        return block(item, half, step, across) if half == 0 else block(item, half, across, step)
+
+    def second_sems(item, half, d, kind):
+        k = ((item * 2 + half) * 2 + d) * 6 + kind
+        return second_send.at[k], second_recv.at[k]
+
+    def second_start(item, *which):
+        for n in which:
+            for half in range(2):
+                for d in range(2):
+                    ref = second_block(item, half, 0, d, n)
+                    send(ref, ref, *second_sems(item, half, d, n), ring_device(half, 1, 1 - 2 * d))
+
+    def second_near(item, *which):
+        for n in which:
+            for half in range(2):
+                for d in range(2):
+                    to = 1 - 2 * d
+                    arrive(second_block(item, half, -to, d, n), *second_sems(item, half, d, n), ring_device(half, 1, to))
+
+    def second_forward(item, *which):
+        for n in which:
+            for half in range(2):
+                for d in range(2):
+                    to = 1 - 2 * d
+                    ref = second_block(item, half, -to, d, n)
+                    arrive(ref, *second_sems(item, half, d, n), ring_device(half, 1, to))
+                    send(ref, ref, *second_sems(item, half, d, 4 + n), ring_device(half, 1, to))
+
+    def second_far(item, *which):
+        for n in which:
+            for half in range(2):
+                for d in range(2):
+                    ref = second_block(item, half, 2, d, n)
+                    arrive(ref, *second_sems(item, half, d, 4 + n), ring_device(half, 1, 1 - 2 * d))
 
     def x_piece(which, t, p):
         if which == 0:
@@ -231,28 +265,28 @@
                 columns = slice(256 * t, 256 * t + 256)
                 wide[rows, columns] = (blocks[t] * scale * gains[gain, :, columns]).astype(BF)
 
-    ring_start(ATTN, 0)
+    first_start(ATTN)
     x_start(0)
-    ring_start(UP, 0)
-    ring_forward(ATTN, 0)
-    ring_near(ATTN, 0)
+    first_start(UP)
+    first_forward(ATTN)
+    first_near(ATTN)
     x_forward(0)
-    ring_far(ATTN, 0)
-    ring_start(ATTN, 1)
-    ring_forward(UP, 0)
+    first_far(ATTN)
+    second_start(ATTN, 0, 1, 2, 3)
+    first_forward(UP)
     x_near(0)
+    second_forward(ATTN, 0, 1)
+    first_start(DOWN)
     x_far(0)
-    ring_forward(ATTN, 1)
-    ring_start(DOWN, 0)
-    ring_near(UP, 0)
-    ring_far(UP, 0)
-    ring_start(UP, 1)
+    first_near(UP)
+    first_far(UP)
+    second_start(UP, 0, 1, 2, 3)
+    second_near(ATTN, 2, 3)
+    second_far(ATTN, 0, 1)
+    x_start(1)
     x_partner(0)
     norm_rows(xall, 0)
-    ring_near(ATTN, 1)
-    ring_far(ATTN, 1)
-    x_start(1)
-    ring_forward(DOWN, 0)
+    first_forward(DOWN)
 
     weights = jnp.concatenate([attn[h, :, :, 0:128, :].reshape(D, 128) for h in range(2)], axis=1)
     qkvg[...] = jnp.dot(wide[...], weights, preferred_element_type=F32)
@@ -285,15 +319,15 @@
     for h in range(2):
         wo[tp, h] = attn[h, :, :, 128:160, :]
     x_forward(1)
-    x_near(1)
     x_forward(2)
     x_near(2)
+    x_near(1)
     x_far(2)
-    ring_forward(UP, 1)
-    ring_near(DOWN, 0)
-    ring_far(DOWN, 0)
-    ring_start(DOWN, 1)
+    second_forward(UP, 0, 1)
     x_far(1)
+    first_near(DOWN)
+    first_far(DOWN)
+    second_start(DOWN, 0, 1, 2)
     x_partner(2)
     x_partner(1)
 
@@ -310,40 +344,124 @@
         mid[t] = (xall[t].astype(F32) + branch).astype(BF)
 
     norm_rows(mid, 1)
-    ring_near(UP, 1)
-    ring_far(UP, 1)
+    second_near(UP, 2, 3)
+    second_far(UP, 0, 1)
+    second_forward(DOWN, 0)
     for h in range(2):
         raw = jnp.dot(wide[...], upb[h].reshape(D, 512), preferred_element_type=F32)
         raw = jnp.maximum(raw, 0.0)
         hid[:, 512 * h : 512 * h + 512] = (raw * raw).astype(BF)
-    ring_forward(DOWN, 1)
-    ring_near(DOWN, 1)
-    ring_far(DOWN, 1)
-
-    def part(t):
-        z0, y0 = lax.div(t, 2), lax.rem(t, 2) * 2
-        total = None
-        for h in range(2):
-            columns = jnp.concatenate([dnb[h, z0, y0], dnb[h, z0, y0 + 1]], axis=1)
-            term = jnp.dot(hid[:, 512 * h : 512 * h + 512], columns, preferred_element_type=F32)
-            total = term if total is None else total + term
-        return total
-
-    for i in (1, 2, 3, 0):
-        pps[i] = part(x_index(i, 1 - core)).astype(BF)
-        send(pps.at[i], ppr.at[i], p_send.at[i], p_recv.at[i], partner)
-    for i in (1, 2, 3, 0):
-        total = part(x_index(i))
-        arrive(ppr.at[i], p_send.at[i], p_recv.at[i], partner)
-        total = total + ppr[i].astype(F32)
-        if i:
-            rss[i - 1] = total.astype(BF)
-            send(rss.at[i - 1], rsr.at[i - 1], r_send.at[i - 1], r_recv.at[i - 1], x_device(i))
-        else:
-            acc[...] = mid[tp].astype(F32) + total
-    for i in range(3):
-        arrive(rsr.at[i], r_send.at[i], r_recv.at[i], x_device(i + 1))
-    out_ref[...] = (acc[...] + rsr[0].astype(F32) + rsr[1].astype(F32) + rsr[2].astype(F32)).astype(BF)
+    second_forward(DOWN, 1)
+    second_start(DOWN, 3)
+
+    def number(dz, dy):
+        return (dz + 1) * 4 + dy + 1
+
+    begun = set()
+
+    def products(pairs):
+        done = []
+        for half, blocks in pairs:
+            columns = jnp.concatenate([block(DOWN, half, dz, dy)[...] for dz, dy in blocks], axis=1)
+            both = jnp.dot(hid[:, 512 * half : 512 * half + 512], columns, preferred_element_type=F32)
+            for k, at in enumerate(blocks):
+                value, n = both[:, 128 * k : 128 * k + 128], number(*at)
+                if at in begun:
+                    acc[n] += value
+                    done.append(at)
+                else:
+                    acc[n] = value
+                    begun.add(at)
+        return done
+
+    def rows_of(c):
+        return pl.ds(pl.multiple_of(c * 192, 64), 192)
+
+    def swap(blocks):
+        for at in blocks:
+            n = number(*at)
+            pps[n] = acc[n, rows_of(1 - core), :].astype(BF)
+            send(pps.at[n], ppr.at[n], p_send.at[n], p_recv.at[n], partner)
+
+    def owner_of(at):
+        z_to, y_to = lax.rem(zl + at[0] + 4, 4), lax.rem(y + at[1] + 4, 4)
+        t = z_to * 2 + lax.div(y_to, 2)
+        k = lax.rem(y_to, 2)
+        n = number(*at)
+        copy = pltpu.make_async_remote_copy(
+            src_ref=rss.at[n], dst_ref=rsr.at[x, k, core], send_sem=r_send.at[n],
+            recv_sem=r_recv.at[(x * 2 + k) * 2 + core], device_id={"tp": t}, device_id_type=MESH,
+        )
+        return t, k, copy
+
+    def deliver(blocks):
+        for at in blocks:
+            n = number(*at)
+            arrive(ppr.at[n], p_send.at[n], p_recv.at[n], partner)
+            total = (acc[n, rows_of(core), :] + ppr[n].astype(F32)).astype(BF)
+            t, k, copy = owner_of(at)
+
+            @pl.when(t == tp)
+            def _():
+                rsr[x, k, core] = total
+
+            @pl.when(t != tp)
+            def _():
+                rss[n] = total
+                copy.start()
+
+    def arrivals(n, far):
+        step = (2, 2) if far else (-1, 1)
+        rows = [(step[d], ORDER[d][n]) for d in range(2)]
+        columns = [(ORDER[d][n], step[d]) for d in range(2)]
+        return [(0, rows), (1, columns)]
+
+    own = [(0, [(0, 0), (0, 1)]), (0, [(0, -1), (0, 2)]), (1, [(0, 0), (1, 0)]), (1, [(-1, 0), (2, 0)])]
+    ready = products(own)
+    swap(ready)
+    more = products(arrivals(0, False))
+    swap(more)
+    deliver(ready)
+    ready = products(arrivals(1, False))
+    swap(ready)
+    deliver(more)
+    second_near(DOWN, 2)
+    more = products(arrivals(2, False))
+    swap(more)
+    deliver(ready)
+    second_far(DOWN, 0)
+    ready = products(arrivals(0, True))
+    swap(ready)
+    deliver(more)
+    second_far(DOWN, 1)
+    more = products(arrivals(1, True))
+    swap(more)
+    deliver(ready)
+    second_near(DOWN, 3)
+    ready = products(arrivals(3, False))
+    swap(ready)
+    deliver(more)
+    deliver(ready)
+
+    def from_chip(step, k, half):
+        other = lax.rem(x + step, 4)
+        arrive(rsr.at[other, k, half], r_send.at[0], r_recv.at[(other * 2 + k) * 2 + half], x_device(1))
+
+    for k in range(2):
+        from_chip(0, k, 1 - core)
+        for step in range(1, 4):
+            for half in range(2):
+                from_chip(step, k, half)
+    for k in range(2):
+        for half in range(2):
+            rows, columns = slice(192 * half, 192 * half + 192), slice(128 * k, 128 * k + 128)
+            total = mid[tp, rows, columns].astype(F32)
+            for chip in range(4):
+                total = total + rsr[chip, k, half].astype(F32)
+            out_ref[rows, columns] = total.astype(BF)
+    for at in sorted(begun):
+        t, _, copy = owner_of(at)
+        pl.when(t != tp)(copy.wait_send)
     for copy in started:
         copy.wait_send()
 
@@ -351,7 +469,7 @@
 def local(activations, norm_gain, qw, kw, vw, gw, ow, mlp_gain, uw, dw):
     cosine, sine = rotary_tables()
     operands = (
-        activations, norm_gain.reshape(1, D), qw, kw, vw, gw, ow, mlp_gain.reshape(1, D), uw, dw,
+        activations, norm_gain.reshape(1, D), qw.T, kw.T, vw.T, gw.T, ow, mlp_gain.reshape(1, D), uw, dw,
         jnp.asarray(cosine), jnp.asarray(sine),
     )
     dma = pltpu.SemaphoreType.DMA
@@ -370,18 +488,18 @@
             pltpu.VMEM((ROWS, D), BF),
             pltpu.VMEM((8, ROWS, 256), BF),
             pltpu.VMEM((ROWS, 1024), BF),
-            pltpu.VMEM((4, ROWS, 256), BF),
-            pltpu.VMEM((4, ROWS, 256), BF),
-            pltpu.VMEM((3, ROWS, 256), BF),
-            pltpu.VMEM((3, ROWS, 256), BF),
-            pltpu.VMEM((4, 128, 64), BF),
+            pltpu.VMEM((16, 192, 128), BF),
+            pltpu.VMEM((16, 192, 128), BF),
+            pltpu.VMEM((16, 192, 128), BF),
+            pltpu.VMEM((4, 2, 2, 192, 128), BF),
+            pltpu.VMEM((4, 64, 128), BF),
             pltpu.VMEM((2, 1, D), F32),
             pltpu.VMEM((2, 128, 128), F32),
             pltpu.VMEM((ROWS, 256), F32),
             pltpu.VMEM((ROWS, 128), F32),
             pltpu.VMEM((ROWS, 512), BF),
-            pltpu.VMEM((ROWS, 256), F32),
-            dma((15,)), dma((72,)), dma((72,)), dma((42,)), dma((42,)), dma((4,)), dma((4,)), dma((3,)), dma((3,)),
+            pltpu.VMEM((16, ROWS, 128), F32),
+            dma((15,)), dma((36,)), dma((36,)), dma((72,)), dma((72,)), dma((42,)), dma((42,)), dma((16,)), dma((16,)), dma((16,)), dma((16,)),
         ],
         compiler_params=pltpu.CompilerParams(
             collective_id=0, has_side_effects=True, vmem_limit_bytes=56 * 1024 * 1024

time: 82.8 us -> 75.6 us (0.913)
  local copies, waits for them, and re-layouts: 5.23 us -> 1.62 us
  Pallas kernels: 77 us -> 73.4 us
    unnamed x11 -> x1, local copies, waits for them, and re-layouts: 5.23 us -> 1.62 us
    pallas_call x1, Pallas kernels: 77 us -> 73.4 us  [local(): pl.pallas_call(layer_kernel, out_shape=jax.ShapeDtypeStruct((ROWS, D // 8...]
where the time goes in v2:
time: 75.6 us; the launch traced here: 75 us
  Pallas kernels  73.4 us (97%)
  local copies, waits for them, and re-layouts  1.62 us (2%)
    pallas_call x1, Pallas kernels, local(): pl.pallas_call(layer_kernel, out_shape=jax.ShapeDtypeStruct((ROWS, D // 8...  73.4 us
    unnamed x1, local copies, waits for them, and re-layouts  1.62 us

profile of v2, /device:TPU:2, one launch (start us, length us, event | category | flops | bytes accessed | tf_op | source)
XLA Modules:
  0.0 75.0 jit_solution(5654783632777028805)
XLA Ops:
  0.0 73.4 %layer.1 = bf16[384,256]{1,0:T(8,128)(2,1)} custom-call(bf16[384,256]{1,0:T(8,128)(2,1)} %act_hbm.1, f32[1,2048]{1,0:T(1,128)} %bitcast.10, bf16[64,128]{1,0:T(8,128)(2,1)} %bitcast.6, bf16[64,128]{1,0:T(8,128)(2,1)} %bitcast.7, bf16[64,128]{1,0:T(8,128)(2,1)} %bitcast.8, bf16[64,128]{1,0:T(8,128)(2,1)} %bitcast.9, bf16[64,128]{1,0:T(8,128)(2,1)} %ow_hbm.1, ...), custom_call_target="tpu_custom_call" | custom-call | tf_op jit(solution)/shard_map/layer/pallas_call | solution.py:476
  73.4 1.6 %copy.14 = bf16[384,256]{1,0:T(8,128)(2,1)} copy(bf16[384,256]{1,0:T(8,128)(2,1)} %layer.1) | data formatting | bytes 393216

commit v3 on v2

--- a/solution.py
+++ b/solution.py
@@ -47,7 +47,7 @@
     out_ref,
     attn, upb, dnb, xall, wo, ret, wide, mid, hid, pps, ppr, rss, rsr,
     small, gains, tables, qkvg, gat, lhs, acc,
-    local_sem, first_send, first_recv, second_send, second_recv, x_send, x_recv, p_send, p_recv, r_send, r_recv,
+    relay, local_sem, ring_send, first_recv, second_recv, x_send, x_recv, p_send, p_recv, r_send, r_recv, relay_recv,
 ):
     rep, fs, tp = lax.axis_index("rep"), lax.axis_index("fs"), lax.axis_index("tp")
     zl, y = lax.div(fs, 4), lax.rem(fs, 4)
@@ -68,6 +68,12 @@
         return {"tp": x_index(step)}
 
     partner = {"tp": x * 2 + (1 - core)}
+
+    barrier = pltpu.get_barrier_semaphore()
+    peers = [y_device(1), y_device(-1), z_device(1), z_device(-1), partner]
+    peers += [{"tp": x_index(step, c)} for step in (1, -1, 2) for c in range(2)]
+    for peer in peers:
+        pl.semaphore_signal(barrier, inc=1, device_id=peer, device_id_type=MESH)
 
     loads = [
         pltpu.make_async_copy(qw_hbm, small.at[0], local_sem.at[0]),
@@ -88,31 +94,25 @@
     ]
     for copy in loads:
         copy.start()
-
-    barrier = pltpu.get_barrier_semaphore()
-    peers = [y_device(1), y_device(-1), z_device(1), z_device(-1), partner]
-    peers += [{"tp": x_index(step, c)} for step in (1, -1, 2) for c in range(2)]
-    for peer in peers:
-        pl.semaphore_signal(barrier, inc=1, device_id=peer, device_id_type=MESH)
-    for copy in loads:
+    for copy in loads[:6]:
         copy.wait()
     for h in range(2):
         attn[h, zl, y, 0:128, :] = small[2 * h : 2 * h + 2].reshape(128, 128).astype(F32).T.astype(BF)
     pl.semaphore_wait(barrier, len(peers))
 
-    started = []
-
-    def send(src, dst, send_sem, recv_sem, device):
-        copy = pltpu.make_async_remote_copy(
+    def remote(src, dst, send_sem, recv_sem, device):
+        return pltpu.make_async_remote_copy(
             src_ref=src, dst_ref=dst, send_sem=send_sem, recv_sem=recv_sem, device_id=device, device_id_type=MESH
         )
-        copy.start()
-        started.append(copy)
-
-    def arrive(region, send_sem, recv_sem, device):
-        pltpu.make_async_remote_copy(
-            src_ref=region, dst_ref=region, send_sem=send_sem, recv_sem=recv_sem, device_id=device, device_id_type=MESH
-        ).wait_recv()
+
+    def send(src, dst, send_sem, recv_sem, device):
+        remote(src, dst, send_sem, recv_sem, device).start()
+
+    def arrive(region, recv_sem):
+        remote(region, region, r_send.at[0], recv_sem, partner).wait_recv()
+
+    def sent(region, send_sem):
+        remote(region, region, send_sem, r_recv.at[0], partner).wait_send()
 
     bufs = (attn, upb, dnb)
     depth = (160, 128, 512)
@@ -131,58 +131,46 @@
     def ring_device(half, phase, step):
         return y_device(step) if along_y(half, phase) else z_device(step)
 
-    def first_sems(item, half, d, kind):
-        k = ((item * 2 + half) * 2 + d) * 3 + kind
-        return first_send.at[k], first_recv.at[k]
+    def first_sem(item, half=2, d=0):
+        return first_recv.at[item * 5 + half * 2 + d]
 
     def first_start(item):
         for n in range(2):
             for half in range(2):
                 for d in range(2):
-                    p = n if d == 0 else 1 - n
-                    ref = piece(item, half, 0, p)
-                    send(ref, ref, *first_sems(item, half, d, n), ring_device(half, 0, 1 - 2 * d))
+                    ref = piece(item, half, 0, n if d == 0 else 1 - n)
+                    sem = first_sem(item, half, d) if n == 0 else first_sem(item)
+                    send(ref, ref, ring_send.at[item], sem, ring_device(half, 0, 1 - 2 * d))
 
     def first_forward(item):
         for half in range(2):
             for d in range(2):
                 to = 1 - 2 * d
                 ref = piece(item, half, -to, d)
-                arrive(ref, *first_sems(item, half, d, 0), ring_device(half, 0, to))
-                send(ref, ref, *first_sems(item, half, d, 2), ring_device(half, 0, to))
-
-    def first_near(item):
-        for half in range(2):
-            for d in range(2):
-                to = 1 - 2 * d
-                arrive(piece(item, half, -to, 1 - d), *first_sems(item, half, d, 1), ring_device(half, 0, to))
-
-    def first_far(item):
-        for half in range(2):
-            for d in range(2):
-                arrive(piece(item, half, 2, d), *first_sems(item, half, d, 2), ring_device(half, 0, 1 - 2 * d))
+                arrive(ref, first_sem(item, half, d))
+                send(ref, ref, ring_send.at[item], first_sem(item), ring_device(half, 0, to))
+
+    def first_rest(item):
+        arrive(bufs[item].at[0, 0], first_sem(item))
 
     def second_block(item, half, step, d, n):
         across = ORDER[d][n]
         return block(item, half, step, across) if half == 0 else block(item, half, across, step)
 
-    def second_sems(item, half, d, kind):
-        k = ((item * 2 + half) * 2 + d) * 6 + kind
-        return second_send.at[k], second_recv.at[k]
+    def second_sem(item, half, d, n, far):
+        if n < 2 and not far:
+            return second_recv.at[item * 8 + half * 4 + d * 2 + n]
+        if item < DOWN:
+            return second_recv.at[24 + item]
+        return second_recv.at[26 + n]
 
     def second_start(item, *which):
         for n in which:
             for half in range(2):
                 for d in range(2):
                     ref = second_block(item, half, 0, d, n)
-                    send(ref, ref, *second_sems(item, half, d, n), ring_device(half, 1, 1 - 2 * d))
-
-    def second_near(item, *which):
-        for n in which:
-            for half in range(2):
-                for d in range(2):
-                    to = 1 - 2 * d
-                    arrive(second_block(item, half, -to, d, n), *second_sems(item, half, d, n), ring_device(half, 1, to))
+                    sem = second_sem(item, half, d, n, False)
+                    send(ref, ref, ring_send.at[3 + item], sem, ring_device(half, 1, 1 - 2 * d))
 
     def second_forward(item, *which):
         for n in which:
@@ -190,15 +178,15 @@
                 for d in range(2):
                     to = 1 - 2 * d
                     ref = second_block(item, half, -to, d, n)
-                    arrive(ref, *second_sems(item, half, d, n), ring_device(half, 1, to))
-                    send(ref, ref, *second_sems(item, half, d, 4 + n), ring_device(half, 1, to))
-
-    def second_far(item, *which):
-        for n in which:
-            for half in range(2):
-                for d in range(2):
-                    ref = second_block(item, half, 2, d, n)
-                    arrive(ref, *second_sems(item, half, d, 4 + n), ring_device(half, 1, 1 - 2 * d))
+                    arrive(ref, second_sem(item, half, d, n, False))
+                    sem = second_sem(item, half, d, n, True)
+                    send(ref, ref, ring_send.at[3 + item], sem, ring_device(half, 1, to))
+
+    def second_rest(item):
+        arrive(bufs[item].at[0], second_sem(item, 0, 0, 0, True))
+
+    def second_four(item, n, far):
+        arrive(bufs[item].at[0, 0], second_sem(item, 0, 0, n, far))
 
     def x_piece(which, t, p):
         if which == 0:
@@ -207,50 +195,47 @@
             return wo.at[t, p]
         return ret.at[t, pl.ds(p * 96, 96)]
 
-    def x_sems(which, kind):
-        k = which * 14 + kind
-        return x_send.at[k], x_recv.at[k]
+    whole = (xall, wo, ret)
+
+    def x_sem(which, kind):
+        return x_recv.at[which * 5 + kind]
 
     def hand_over(which, place, p):
         ref = x_piece(which, x_index((0, -1, 1, 2)[place]), p)
-        send(ref, ref, *x_sems(which, 6 + 2 * place + p), partner)
+        send(ref, ref, x_send.at[which], x_sem(which, 4), partner)
 
     def x_start(which):
-        for p in range(2):
+        for n in range(2):
             for d in range(2):
-                q = p if d == 0 else 1 - p
-                dst = x_piece(which, tp, q)
-                src = attn.at[q, :, :, pl.ds(128, 32)] if which == 1 else dst
-                send(src, dst, *x_sems(which, 2 * d + q), x_device(1 - 2 * d))
+                p = n if d == 0 else 1 - n
+                dst = x_piece(which, tp, p)
+                src = attn.at[p, :, :, pl.ds(128, 32)] if which == 1 else dst
+                send(src, dst, x_send.at[which], x_sem(which, d if n == 0 else 2), x_device(1 - 2 * d))
         for p in range(2):
             dst = x_piece(which, tp, p)
             src = attn.at[p, :, :, pl.ds(128, 32)] if which == 1 else dst
-            send(src, dst, *x_sems(which, 6 + p), partner)
+            send(src, dst, x_send.at[which], x_sem(which, 4), partner)
 
     def x_forward(which):
         for d in range(2):
             to = 1 - 2 * d
             ref = x_piece(which, x_index(-to), d)
-            arrive(ref, *x_sems(which, 2 * d + d), x_device(to))
-            send(ref, ref, *x_sems(which, 4 + d), x_device(to))
+            arrive(ref, x_sem(which, d))
+            send(ref, ref, x_send.at[which], x_sem(which, 3), x_device(to))
             hand_over(which, 1 + d, d)
 
     def x_near(which):
+        arrive(whole[which].at[0], x_sem(which, 2))
         for d in range(2):
-            to = 1 - 2 * d
-            arrive(x_piece(which, x_index(-to), 1 - d), *x_sems(which, 2 * d + 1 - d), x_device(to))
             hand_over(which, 1 + d, 1 - d)
 
     def x_far(which):
+        arrive(whole[which].at[0], x_sem(which, 3))
         for d in range(2):
-            arrive(x_piece(which, x_index(2), d), *x_sems(which, 4 + d), x_device(1 - 2 * d))
             hand_over(which, 3, d)
 
     def x_partner(which):
-        for place in range(4):
-            t = x_index((0, -1, 1, 2)[place], 1 - core)
-            for p in range(2):
-                arrive(x_piece(which, t, p), *x_sems(which, 6 + 2 * place + p), partner)
+        arrive(whole[which].at[pl.ds(0, 4)], x_sem(which, 4))
 
     def norm_rows(source, gain):
         @pl.loop(0, ROWS // 16)
@@ -266,27 +251,30 @@
                 wide[rows, columns] = (blocks[t] * scale * gains[gain, :, columns]).astype(BF)
 
     first_start(ATTN)
+    loads[6].wait()
     x_start(0)
+    loads[7].wait()
+    loads[8].wait()
     first_start(UP)
+    for copy in loads[9:]:
+        copy.wait()
     first_forward(ATTN)
-    first_near(ATTN)
     x_forward(0)
-    first_far(ATTN)
+    first_forward(UP)
+    first_rest(ATTN)
     second_start(ATTN, 0, 1, 2, 3)
-    first_forward(UP)
     x_near(0)
     second_forward(ATTN, 0, 1)
     first_start(DOWN)
     x_far(0)
-    first_near(UP)
-    first_far(UP)
-    second_start(UP, 0, 1, 2, 3)
-    second_near(ATTN, 2, 3)
-    second_far(ATTN, 0, 1)
-    x_start(1)
     x_partner(0)
     norm_rows(xall, 0)
+    first_rest(UP)
+    second_start(UP, 0)
+    second_rest(ATTN)
+    x_start(1)
     first_forward(DOWN)
+    second_start(UP, 1, 2, 3)
 
     weights = jnp.concatenate([attn[h, :, :, 0:128, :].reshape(D, 128) for h in range(2)], axis=1)
     qkvg[...] = jnp.dot(wide[...], weights, preferred_element_type=F32)
@@ -325,9 +313,8 @@
     x_far(2)
     second_forward(UP, 0, 1)
     x_far(1)
-    first_near(DOWN)
-    first_far(DOWN)
-    second_start(DOWN, 0, 1, 2)
+    first_rest(DOWN)
+    second_start(DOWN, 0, 1)
     x_partner(2)
     x_partner(1)
 
@@ -344,15 +331,12 @@
         mid[t] = (xall[t].astype(F32) + branch).astype(BF)
 
     norm_rows(mid, 1)
-    second_near(UP, 2, 3)
-    second_far(UP, 0, 1)
-    second_forward(DOWN, 0)
+    second_rest(UP)
     for h in range(2):
         raw = jnp.dot(wide[...], upb[h].reshape(D, 512), preferred_element_type=F32)
         raw = jnp.maximum(raw, 0.0)
         hid[:, 512 * h : 512 * h + 512] = (raw * raw).astype(BF)
-    second_forward(DOWN, 1)
-    second_start(DOWN, 3)
+    second_forward(DOWN, 0)
 
     def number(dz, dy):
         return (dz + 1) * 4 + dy + 1
@@ -377,38 +361,61 @@
     def rows_of(c):
         return pl.ds(pl.multiple_of(c * 192, 64), 192)
 
-    def swap(blocks):
+    def swap(blocks, group):
         for at in blocks:
             n = number(*at)
             pps[n] = acc[n, rows_of(1 - core), :].astype(BF)
-            send(pps.at[n], ppr.at[n], p_send.at[n], p_recv.at[n], partner)
-
-    def owner_of(at):
+            send(pps.at[n], ppr.at[n], p_send.at[0], p_recv.at[group], partner)
+
+    way = 1 - 2 * core
+
+    def route(at):
         z_to, y_to = lax.rem(zl + at[0] + 4, 4), lax.rem(y + at[1] + 4, 4)
-        t = z_to * 2 + lax.div(y_to, 2)
-        k = lax.rem(y_to, 2)
-        n = number(*at)
-        copy = pltpu.make_async_remote_copy(
-            src_ref=rss.at[n], dst_ref=rsr.at[x, k, core], send_sem=r_send.at[n],
-            recv_sem=r_recv.at[(x * 2 + k) * 2 + core], device_id={"tp": t}, device_id_type=MESH,
-        )
-        return t, k, copy
-
-    def deliver(blocks):
+        c_to, k = lax.div(y_to, 2), lax.rem(y_to, 2)
+        hops = lax.rem(way * (z_to - x) + 8, 4)
+        return number(*at), {"tp": z_to * 2 + c_to}, c_to, k, hops
+
+    def deliver(blocks, group):
+        arrive(ppr.at[pl.ds(0, len(blocks))], p_recv.at[group])
         for at in blocks:
-            n = number(*at)
-            arrive(ppr.at[n], p_send.at[n], p_recv.at[n], partner)
+            n, owner, c_to, k, hops = route(at)
             total = (acc[n, rows_of(core), :] + ppr[n].astype(F32)).astype(BF)
-            t, k, copy = owner_of(at)
-
-            @pl.when(t == tp)
+            rss[n] = total
+
+            if group < 5:
+
+                @pl.when(hops == 2)
+                def _():
+                    send(rss.at[n], relay.at[at[1] + 1], r_send.at[0], relay_recv.at[at[1] + 1], x_device(way))
+
+                @pl.when((hops == 3) | ((hops == 0) & (c_to != core)))
+                def _():
+                    send(rss.at[n], rsr.at[hops, k, core], r_send.at[0], r_recv.at[0], owner)
+
+            else:
+
+                @pl.when(hops == 2)
+                def _():
+                    send(rss.at[n], rsr.at[2, k, core], r_send.at[0], r_recv.at[1 + k], owner)
+
+                @pl.when((hops % 2 == 1) | ((hops == 0) & (c_to != core)))
+                def _():
+                    send(rss.at[n], rsr.at[hops, k, core], r_send.at[0], r_recv.at[0], owner)
+
+            @pl.when((hops == 0) & (c_to == core))
             def _():
-                rsr[x, k, core] = total
-
-            @pl.when(t != tp)
+                rsr[0, k, core] = total
+
+    def pass_on(blocks):
+        for at in blocks:
+            n, owner, _, k, hops = route(at)
+
+            @pl.when(hops == 1)
             def _():
-                rss[n] = total
-                copy.start()
+                arrive(relay.at[at[1] + 1], relay_recv.at[at[1] + 1])
+                total = acc[n, rows_of(core), :] + ppr[n].astype(F32) + relay[at[1] + 1].astype(F32)
+                rss[n] = total.astype(BF)
+                send(rss.at[n], rsr.at[1, k, core], r_send.at[0], r_recv.at[0], owner)
 
     def arrivals(n, far):
         step = (2, 2) if far else (-1, 1)
@@ -417,53 +424,81 @@
         return [(0, rows), (1, columns)]
 
     own = [(0, [(0, 0), (0, 1)]), (0, [(0, -1), (0, 2)]), (1, [(0, 0), (1, 0)]), (1, [(-1, 0), (2, 0)])]
-    ready = products(own)
-    swap(ready)
-    more = products(arrivals(0, False))
-    swap(more)
-    deliver(ready)
-    ready = products(arrivals(1, False))
-    swap(ready)
-    deliver(more)
-    second_near(DOWN, 2)
-    more = products(arrivals(2, False))
-    swap(more)
-    deliver(ready)
-    second_far(DOWN, 0)
-    ready = products(arrivals(0, True))
-    swap(ready)
-    deliver(more)
-    second_far(DOWN, 1)
-    more = products(arrivals(1, True))
-    swap(more)
-    deliver(ready)
-    second_near(DOWN, 3)
-    ready = products(arrivals(3, False))
-    swap(ready)
-    deliver(more)
-    deliver(ready)
-
-    def from_chip(step, k, half):
-        other = lax.rem(x + step, 4)
-        arrive(rsr.at[other, k, half], r_send.at[0], r_recv.at[(other * 2 + k) * 2 + half], x_device(1))
+    s0 = products(own)
+    swap(s0, 0)
+    s1 = products(arrivals(0, False))
+    swap(s1, 1)
+    deliver(s0, 0)
+    second_forward(DOWN, 1)
+    second_start(DOWN, 2, 3)
+    s2 = products(arrivals(1, False))
+    swap(s2, 2)
+    deliver(s1, 1)
+    deliver(s2, 2)
+    second_four(DOWN, 0, True)
+    s3 = products(arrivals(0, True))
+    swap(s3, 3)
+    pass_on(s0)
+    deliver(s3, 3)
+    second_four(DOWN, 1, True)
+    s4 = products(arrivals(1, True))
+    swap(s4, 4)
+    pass_on(s1)
+    pass_on(s2)
+    deliver(s4, 4)
+    second_four(DOWN, 2, False)
+    s5 = products(arrivals(2, False))
+    swap(s5, 5)
+    pass_on(s3)
+    deliver(s5, 5)
+    second_four(DOWN, 3, False)
+    s6 = products(arrivals(3, False))
+    swap(s6, 6)
+    deliver(s6, 6)
+    pass_on(s4)
+
+    def straight(k):
+        dz, dy = lax.rem(x - zl + 4, 4), lax.rem(core * 2 + k - y + 4, 4)
+        found = (dz == 0) & (dy < 0)
+        for at in s5 + s6:
+            found = found | ((dz == at[0] % 4) & (dy == at[1] % 4))
+        return found
 
     for k in range(2):
-        from_chip(0, k, 1 - core)
-        for step in range(1, 4):
+
+        @pl.when(jnp.logical_not(straight(k)))
+        def _():
+            rsr[2, k] = jnp.zeros((2, 192, 128), BF)
+
+    def collect():
+        arrive(rss.at[pl.ds(0, 10)], r_recv.at[0])
+        for k in range(2):
+
+            @pl.when(straight(k))
+            def _():
+                arrive(rss.at[pl.ds(0, 2)], r_recv.at[1 + k])
+
+    def finish():
+        for k in range(2):
             for half in range(2):
-                from_chip(step, k, half)
-    for k in range(2):
-        for half in range(2):
-            rows, columns = slice(192 * half, 192 * half + 192), slice(128 * k, 128 * k + 128)
-            total = mid[tp, rows, columns].astype(F32)
-            for chip in range(4):
-                total = total + rsr[chip, k, half].astype(F32)
-            out_ref[rows, columns] = total.astype(BF)
-    for at in sorted(begun):
-        t, _, copy = owner_of(at)
-        pl.when(t != tp)(copy.wait_send)
-    for copy in started:
-        copy.wait_send()
+                rows, columns = slice(192 * half, 192 * half + 192), slice(128 * k, 128 * k + 128)
+                total = mid[tp, rows, columns].astype(F32)
+                for hops in range(4):
+                    total = total + rsr[hops, k, half].astype(F32)
+                out_ref[rows, columns] = total.astype(BF)
+
+    def drain():
+        for item in range(3):
+            sent(bufs[item].at[:, pl.ds(0, 3), 0], ring_send.at[item])
+            sent(bufs[item].at[:, pl.ds(0, 3)], ring_send.at[3 + item])
+        for which in range(3):
+            sent(whole[which].at[pl.ds(0, 7)], x_send.at[which])
+        sent(pps, p_send.at[0])
+        sent(rss.at[pl.ds(0, 14)], r_send.at[0])
+
+    collect()
+    finish()
+    drain()
 
 
 def local(activations, norm_gain, qw, kw, vw, gw, ow, mlp_gain, uw, dw):
@@ -473,9 +508,9 @@
         jnp.asarray(cosine), jnp.asarray(sine),
     )
     dma = pltpu.SemaphoreType.DMA
-    return pl.pallas_call(
+    rows = pl.pallas_call(
         layer_kernel,
-        out_shape=jax.ShapeDtypeStruct((ROWS, D // 8), BF),
+        out_shape=pltpu.VMEM((ROWS, D // 8), BF),
         in_specs=[pl.BlockSpec(memory_space=pltpu.HBM)] * len(operands),
         out_specs=pl.BlockSpec(memory_space=pltpu.VMEM),
         scratch_shapes=[
@@ -499,13 +534,15 @@
             pltpu.VMEM((ROWS, 128), F32),
             pltpu.VMEM((ROWS, 512), BF),
             pltpu.VMEM((16, ROWS, 128), F32),
-            dma((15,)), dma((36,)), dma((36,)), dma((72,)), dma((72,)), dma((42,)), dma((42,)), dma((16,)), dma((16,)), dma((16,)), dma((16,)),
+            pltpu.VMEM((4, 192, 128), BF),
+            dma((15,)), dma((6,)), dma((15,)), dma((30,)), dma((3,)), dma((15,)), dma((1,)), dma((7,)), dma((1,)), dma((3,)), dma((4,)),
         ],
         compiler_params=pltpu.CompilerParams(
             collective_id=0, has_side_effects=True, vmem_limit_bytes=56 * 1024 * 1024
         ),
         name="layer",
     )(*operands)
+    return rows
 
 
 def solution(mesh):

time: 75.6 us -> 70.1 us (0.927)
  Pallas kernels: 73.4 us -> 69.2 us
  local copies, waits for them, and re-layouts: 1.62 us -> 0.68 us
    pallas_call x1, Pallas kernels: 73.4 us -> 69.2 us  [local(): pl.pallas_call(layer_kernel, out_shape=pltpu.VMEM((ROWS, D // 8), BF), in...]
    unnamed x1, local copies, waits for them, and re-layouts: 1.62 us -> 0.68 us
where the time goes in v3:
time: 70.1 us; the launch traced here: 69.9 us
  Pallas kernels  69.2 us (99%)
    pallas_call x1, Pallas kernels, local(): pl.pallas_call(layer_kernel, out_shape=pltpu.VMEM((ROWS, D // 8), BF), in...  69.2 us

profile of v3, /device:TPU:2, one launch (start us, length us, event | category | flops | bytes accessed | tf_op | source)
XLA Modules:
  0.0 69.9 jit_solution(7343248857583889098)
XLA Ops:
  0.0 69.2 %layer.1 = bf16[384,256]{1,0:T(8,128)(2,1)S(1)} custom-call(bf16[384,256]{1,0:T(8,128)(2,1)} %act_hbm.1, f32[1,2048]{1,0:T(1,128)} %bitcast.10, bf16[64,128]{1,0:T(8,128)(2,1)} %bitcast.6, bf16[64,128]{1,0:T(8,128)(2,1)} %bitcast.7, bf16[64,128]{1,0:T(8,128)(2,1)} %bitcast.8, bf16[64,128]{1,0:T(8,128)(2,1)} %bitcast.9, bf16[64,128]{1,0:T(8,128)(2,1)} %ow_hbm.1, ...), custom_call_target="tpu_custom_call" | custom-call | tf_op jit(solution)/shard_map/layer/pallas_call | solution.py:511
  69.2 0.7 copy.14

commit v4 on v3

--- a/solution.py
+++ b/solution.py
@@ -17,7 +17,7 @@
 F32 = jnp.float32
 MESH = pl.DeviceIdType.MESH
 ATTN, UP, DOWN = 0, 1, 2
-ORDER = ((0, 1, -1, 2), (-1, 2, 0, 1))
+ORDER = ((0, 1, 2, -1), (-1, 2, 0, 1))
 
 
 def rotary_tables():
@@ -47,7 +47,7 @@
     out_ref,
     attn, upb, dnb, xall, wo, ret, wide, mid, hid, pps, ppr, rss, rsr,
     small, gains, tables, qkvg, gat, lhs, acc,
-    relay, local_sem, ring_send, first_recv, second_recv, x_send, x_recv, p_send, p_recv, r_send, r_recv, relay_recv,
+    local_sem, ring_send, first_recv, second_recv, x_send, x_recv, p_send, p_recv, r_send, r_recv,
 ):
     rep, fs, tp = lax.axis_index("rep"), lax.axis_index("fs"), lax.axis_index("tp")
     zl, y = lax.div(fs, 4), lax.rem(fs, 4)
@@ -75,27 +75,31 @@
     for peer in peers:
         pl.semaphore_signal(barrier, inc=1, device_id=peer, device_id_type=MESH)
 
-    loads = [
-        pltpu.make_async_copy(qw_hbm, small.at[0], local_sem.at[0]),
-        pltpu.make_async_copy(kw_hbm, small.at[1], local_sem.at[1]),
-        pltpu.make_async_copy(vw_hbm, small.at[2], local_sem.at[2]),
-        pltpu.make_async_copy(gw_hbm, small.at[3], local_sem.at[3]),
-        pltpu.make_async_copy(ow_hbm.at[pl.ds(0, 32)], attn.at[0, zl, y, pl.ds(128, 32)], local_sem.at[4]),
-        pltpu.make_async_copy(ow_hbm.at[pl.ds(32, 32)], attn.at[1, zl, y, pl.ds(128, 32)], local_sem.at[5]),
-        pltpu.make_async_copy(act_hbm, xall.at[tp], local_sem.at[6]),
-        pltpu.make_async_copy(uw_hbm.at[:, pl.ds(0, 512)], upb.at[0, zl, y], local_sem.at[7]),
-        pltpu.make_async_copy(uw_hbm.at[:, pl.ds(512, 512)], upb.at[1, zl, y], local_sem.at[8]),
-        pltpu.make_async_copy(dw_hbm.at[pl.ds(0, 512)], dnb.at[0, zl, y], local_sem.at[9]),
-        pltpu.make_async_copy(dw_hbm.at[pl.ds(512, 512)], dnb.at[1, zl, y], local_sem.at[10]),
-        pltpu.make_async_copy(ng_hbm, gains.at[0], local_sem.at[11]),
-        pltpu.make_async_copy(mg_hbm, gains.at[1], local_sem.at[12]),
-        pltpu.make_async_copy(cos_hbm, tables.at[0], local_sem.at[13]),
-        pltpu.make_async_copy(sin_hbm, tables.at[1], local_sem.at[14]),
-    ]
-    for copy in loads:
-        copy.start()
-    for copy in loads[:6]:
-        copy.wait()
+    loads = (
+        (qw_hbm, small.at[0], 0),
+        (kw_hbm, small.at[1], 0),
+        (vw_hbm, small.at[2], 0),
+        (gw_hbm, small.at[3], 0),
+        (ow_hbm.at[pl.ds(0, 32)], attn.at[0, zl, y, pl.ds(128, 32)], 1),
+        (ow_hbm.at[pl.ds(32, 32)], attn.at[1, zl, y, pl.ds(128, 32)], 1),
+        (act_hbm, xall.at[tp], 2),
+        (uw_hbm.at[:, pl.ds(0, 512)], upb.at[0, zl, y], 3),
+        (uw_hbm.at[:, pl.ds(512, 512)], upb.at[1, zl, y], 3),
+        (dw_hbm.at[pl.ds(0, 512)], dnb.at[0, zl, y], 4),
+        (dw_hbm.at[pl.ds(512, 512)], dnb.at[1, zl, y], 4),
+        (ng_hbm, gains.at[0], 5),
+        (mg_hbm, gains.at[1], 5),
+        (cos_hbm, tables.at[0], 6),
+        (sin_hbm, tables.at[1], 6),
+    )
+    for src, dst, n in loads:
+        pltpu.make_async_copy(src, dst, local_sem.at[n]).start()
+
+    def loaded(region, n):
+        pltpu.make_async_copy(region, region, local_sem.at[n]).wait()
+
+    loaded(small, 0)
+    loaded(attn.at[0, 0, 0, pl.ds(0, 64)], 1)
     for h in range(2):
         attn[h, zl, y, 0:128, :] = small[2 * h : 2 * h + 2].reshape(128, 128).astype(F32).T.astype(BF)
     pl.semaphore_wait(barrier, len(peers))
@@ -130,63 +134,55 @@
 
     def ring_device(half, phase, step):
         return y_device(step) if along_y(half, phase) else z_device(step)
-
-    def first_sem(item, half=2, d=0):
-        return first_recv.at[item * 5 + half * 2 + d]
 
     def first_start(item):
         for n in range(2):
             for half in range(2):
                 for d in range(2):
                     ref = piece(item, half, 0, n if d == 0 else 1 - n)
-                    sem = first_sem(item, half, d) if n == 0 else first_sem(item)
-                    send(ref, ref, ring_send.at[item], sem, ring_device(half, 0, 1 - 2 * d))
+                    send(ref, ref, ring_send.at[item], first_recv.at[2 * item + n], ring_device(half, 0, 1 - 2 * d))
 
     def first_forward(item):
+        arrive(bufs[item].at[0, 0, pl.ds(0, 2)], first_recv.at[2 * item])
         for half in range(2):
             for d in range(2):
                 to = 1 - 2 * d
                 ref = piece(item, half, -to, d)
-                arrive(ref, first_sem(item, half, d))
-                send(ref, ref, ring_send.at[item], first_sem(item), ring_device(half, 0, to))
+                send(ref, ref, ring_send.at[item], first_recv.at[2 * item + 1], ring_device(half, 0, to))
 
     def first_rest(item):
-        arrive(bufs[item].at[0, 0], first_sem(item))
+        arrive(bufs[item].at[0, 0], first_recv.at[2 * item + 1])
 
     def second_block(item, half, step, d, n):
         across = ORDER[d][n]
         return block(item, half, step, across) if half == 0 else block(item, half, across, step)
 
-    def second_sem(item, half, d, n, far):
+    def second_sem(item, n, far):
         if n < 2 and not far:
-            return second_recv.at[item * 8 + half * 4 + d * 2 + n]
-        if item < DOWN:
-            return second_recv.at[24 + item]
-        return second_recv.at[26 + n]
+            return second_recv.at[2 * item + n]
+        return second_recv.at[6 + item] if item < DOWN else second_recv.at[8 + n]
 
     def second_start(item, *which):
         for n in which:
             for half in range(2):
                 for d in range(2):
                     ref = second_block(item, half, 0, d, n)
-                    sem = second_sem(item, half, d, n, False)
-                    send(ref, ref, ring_send.at[3 + item], sem, ring_device(half, 1, 1 - 2 * d))
+                    send(ref, ref, ring_send.at[3 + item], second_sem(item, n, False), ring_device(half, 1, 1 - 2 * d))
 
     def second_forward(item, *which):
         for n in which:
+            arrive(bufs[item].at[0, 0], second_sem(item, n, False))
             for half in range(2):
                 for d in range(2):
                     to = 1 - 2 * d
                     ref = second_block(item, half, -to, d, n)
-                    arrive(ref, second_sem(item, half, d, n, False))
-                    sem = second_sem(item, half, d, n, True)
-                    send(ref, ref, ring_send.at[3 + item], sem, ring_device(half, 1, to))
+                    send(ref, ref, ring_send.at[3 + item], second_sem(item, n, True), ring_device(half, 1, to))
 
     def second_rest(item):
-        arrive(bufs[item].at[0], second_sem(item, 0, 0, 0, True))
+        arrive(bufs[item].at[0], second_sem(item, 0, True))
 
     def second_four(item, n, far):
-        arrive(bufs[item].at[0, 0], second_sem(item, 0, 0, n, far))
+        arrive(bufs[item].at[0, 0], second_sem(item, n, far))
 
     def x_piece(which, t, p):
         if which == 0:
@@ -198,11 +194,11 @@
     whole = (xall, wo, ret)
 
     def x_sem(which, kind):
-        return x_recv.at[which * 5 + kind]
+        return x_recv.at[which * 4 + kind]
 
     def hand_over(which, place, p):
         ref = x_piece(which, x_index((0, -1, 1, 2)[place]), p)
-        send(ref, ref, x_send.at[which], x_sem(which, 4), partner)
+        send(ref, ref, x_send.at[which], x_sem(which, 3), partner)
 
     def x_start(which):
         for n in range(2):
@@ -210,32 +206,32 @@
                 p = n if d == 0 else 1 - n
                 dst = x_piece(which, tp, p)
                 src = attn.at[p, :, :, pl.ds(128, 32)] if which == 1 else dst
-                send(src, dst, x_send.at[which], x_sem(which, d if n == 0 else 2), x_device(1 - 2 * d))
+                send(src, dst, x_send.at[which], x_sem(which, n), x_device(1 - 2 * d))
         for p in range(2):
             dst = x_piece(which, tp, p)
             src = attn.at[p, :, :, pl.ds(128, 32)] if which == 1 else dst
-            send(src, dst, x_send.at[which], x_sem(which, 4), partner)
+            send(src, dst, x_send.at[which], x_sem(which, 3), partner)
 
     def x_forward(which):
+        arrive(whole[which].at[0], x_sem(which, 0))
         for d in range(2):
             to = 1 - 2 * d
             ref = x_piece(which, x_index(-to), d)
-            arrive(ref, x_sem(which, d))
-            send(ref, ref, x_send.at[which], x_sem(which, 3), x_device(to))
+            send(ref, ref, x_send.at[which], x_sem(which, 2), x_device(to))
             hand_over(which, 1 + d, d)
 
     def x_near(which):
+        arrive(whole[which].at[0], x_sem(which, 1))
+        for d in range(2):
+            hand_over(which, 1 + d, 1 - d)
+
+    def x_far(which):
         arrive(whole[which].at[0], x_sem(which, 2))
         for d in range(2):
-            hand_over(which, 1 + d, 1 - d)
-
-    def x_far(which):
-        arrive(whole[which].at[0], x_sem(which, 3))
-        for d in range(2):
             hand_over(which, 3, d)
 
     def x_partner(which):
-        arrive(whole[which].at[pl.ds(0, 4)], x_sem(which, 4))
+        arrive(whole[which].at[pl.ds(0, 4)], x_sem(which, 3))
 
     def norm_rows(source, gain):
         @pl.loop(0, ROWS // 16)
@@ -251,21 +247,21 @@
                 wide[rows, columns] = (blocks[t] * scale * gains[gain, :, columns]).astype(BF)
 
     first_start(ATTN)
-    loads[6].wait()
+    loaded(xall.at[0], 2)
     x_start(0)
-    loads[7].wait()
-    loads[8].wait()
+    loaded(upb.at[0, 0, pl.ds(0, 2)], 3)
     first_start(UP)
-    for copy in loads[9:]:
-        copy.wait()
+    loaded(dnb.at[0, 0, pl.ds(0, 2)], 4)
+    loaded(gains, 5)
+    loaded(tables, 6)
     first_forward(ATTN)
+    first_forward(UP)
     x_forward(0)
-    first_forward(UP)
     first_rest(ATTN)
     second_start(ATTN, 0, 1, 2, 3)
+    first_start(DOWN)
     x_near(0)
     second_forward(ATTN, 0, 1)
-    first_start(DOWN)
     x_far(0)
     x_partner(0)
     norm_rows(xall, 0)
@@ -367,12 +363,11 @@
             pps[n] = acc[n, rows_of(1 - core), :].astype(BF)
             send(pps.at[n], ppr.at[n], p_send.at[0], p_recv.at[group], partner)
 
-    way = 1 - 2 * core
 
     def route(at):
         z_to, y_to = lax.rem(zl + at[0] + 4, 4), lax.rem(y + at[1] + 4, 4)
         c_to, k = lax.div(y_to, 2), lax.rem(y_to, 2)
-        hops = lax.rem(way * (z_to - x) + 8, 4)
+        hops = lax.rem(z_to - x + 4, 4)
         return number(*at), {"tp": z_to * 2 + c_to}, c_to, k, hops
 
     def deliver(blocks, group):
@@ -382,40 +377,13 @@
             total = (acc[n, rows_of(core), :] + ppr[n].astype(F32)).astype(BF)
             rss[n] = total
 
-            if group < 5:
-
-                @pl.when(hops == 2)
-                def _():
-                    send(rss.at[n], relay.at[at[1] + 1], r_send.at[0], relay_recv.at[at[1] + 1], x_device(way))
-
-                @pl.when((hops == 3) | ((hops == 0) & (c_to != core)))
-                def _():
-                    send(rss.at[n], rsr.at[hops, k, core], r_send.at[0], r_recv.at[0], owner)
-
-            else:
-
-                @pl.when(hops == 2)
-                def _():
-                    send(rss.at[n], rsr.at[2, k, core], r_send.at[0], r_recv.at[1 + k], owner)
-
-                @pl.when((hops % 2 == 1) | ((hops == 0) & (c_to != core)))
-                def _():
-                    send(rss.at[n], rsr.at[hops, k, core], r_send.at[0], r_recv.at[0], owner)
+            @pl.when((hops > 0) | (c_to != core))
+            def _():
+                send(rss.at[n], rsr.at[hops, k, core], r_send.at[0], r_recv.at[0], owner)
 
             @pl.when((hops == 0) & (c_to == core))
             def _():
                 rsr[0, k, core] = total
-
-    def pass_on(blocks):
-        for at in blocks:
-            n, owner, _, k, hops = route(at)
-
-            @pl.when(hops == 1)
-            def _():
-                arrive(relay.at[at[1] + 1], relay_recv.at[at[1] + 1])
-                total = acc[n, rows_of(core), :] + ppr[n].astype(F32) + relay[at[1] + 1].astype(F32)
-                rss[n] = total.astype(BF)
-                send(rss.at[n], rsr.at[1, k, core], r_send.at[0], r_recv.at[0], owner)
 
     def arrivals(n, far):
         step = (2, 2) if far else (-1, 1)
@@ -424,6 +392,11 @@
         return [(0, rows), (1, columns)]
 
     own = [(0, [(0, 0), (0, 1)]), (0, [(0, -1), (0, 2)]), (1, [(0, 0), (1, 0)]), (1, [(-1, 0), (2, 0)])]
+    def deliver_on(c, blocks, group):
+        @pl.when(core == c)
+        def _():
+            deliver(blocks, group)
+
     s0 = products(own)
     swap(s0, 0)
     s1 = products(arrivals(0, False))
@@ -434,49 +407,29 @@
     s2 = products(arrivals(1, False))
     swap(s2, 2)
     deliver(s1, 1)
-    deliver(s2, 2)
+    deliver_on(0, s2, 2)
     second_four(DOWN, 0, True)
     s3 = products(arrivals(0, True))
     swap(s3, 3)
-    pass_on(s0)
-    deliver(s3, 3)
+    deliver_on(1, s2, 2)
+    deliver_on(0, s3, 3)
     second_four(DOWN, 1, True)
     s4 = products(arrivals(1, True))
     swap(s4, 4)
-    pass_on(s1)
-    pass_on(s2)
-    deliver(s4, 4)
+    deliver_on(1, s3, 3)
+    deliver_on(0, s4, 4)
     second_four(DOWN, 2, False)
     s5 = products(arrivals(2, False))
     swap(s5, 5)
-    pass_on(s3)
+    deliver_on(1, s4, 4)
     deliver(s5, 5)
     second_four(DOWN, 3, False)
     s6 = products(arrivals(3, False))
     swap(s6, 6)
     deliver(s6, 6)
-    pass_on(s4)
-
-    def straight(k):
-        dz, dy = lax.rem(x - zl + 4, 4), lax.rem(core * 2 + k - y + 4, 4)
-        found = (dz == 0) & (dy < 0)
-        for at in s5 + s6:
-            found = found | ((dz == at[0] % 4) & (dy == at[1] % 4))
-        return found
-
-    for k in range(2):
-
-        @pl.when(jnp.logical_not(straight(k)))
-        def _():
-            rsr[2, k] = jnp.zeros((2, 192, 128), BF)
 
     def collect():
-        arrive(rss.at[pl.ds(0, 10)], r_recv.at[0])
-        for k in range(2):
-
-            @pl.when(straight(k))
-            def _():
-                arrive(rss.at[pl.ds(0, 2)], r_recv.at[1 + k])
+        arrive(rss.at[pl.ds(0, 14)], r_recv.at[0])
 
     def finish():
         for k in range(2):
@@ -534,8 +487,7 @@
             pltpu.VMEM((ROWS, 128), F32),
             pltpu.VMEM((ROWS, 512), BF),
             pltpu.VMEM((16, ROWS, 128), F32),
-            pltpu.VMEM((4, 192, 128), BF),
-            dma((15,)), dma((6,)), dma((15,)), dma((30,)), dma((3,)), dma((15,)), dma((1,)), dma((7,)), dma((1,)), dma((3,)), dma((4,)),
+            dma((7,)), dma((6,)), dma((6,)), dma((12,)), dma((3,)), dma((12,)), dma((1,)), dma((7,)), dma((1,)), dma((1,)),
         ],
         compiler_params=pltpu.CompilerParams(
             collective_id=0, has_side_effects=True, vmem_limit_bytes=56 * 1024 * 1024

time: 70.1 us -> 68.7 us (0.980)
  Pallas kernels: 69.2 us -> 67.9 us
    pallas_call x1, Pallas kernels: 69.2 us -> 67.9 us  [local(): pl.pallas_call(layer_kernel, out_shape=pltpu.VMEM((ROWS, D // 8), BF), in...]
where the time goes in v4:
time: 68.7 us; the launch traced here: 68.6 us
  Pallas kernels  67.9 us (99%)
    pallas_call x1, Pallas kernels, local(): pl.pallas_call(layer_kernel, out_shape=pltpu.VMEM((ROWS, D // 8), BF), in...  67.9 us

profile of v4, /device:TPU:2, one launch (start us, length us, event | category | flops | bytes accessed | tf_op | source)
XLA Modules:
  0.0 68.6 jit_solution(9604345074039201805)
XLA Ops:
  0.0 67.9 %layer.1 = bf16[384,256]{1,0:T(8,128)(2,1)S(1)} custom-call(bf16[384,256]{1,0:T(8,128)(2,1)} %act_hbm.1, f32[1,2048]{1,0:T(1,128)} %bitcast.10, bf16[64,128]{1,0:T(8,128)(2,1)} %bitcast.6, bf16[64,128]{1,0:T(8,128)(2,1)} %bitcast.7, bf16[64,128]{1,0:T(8,128)(2,1)} %bitcast.8, bf16[64,128]{1,0:T(8,128)(2,1)} %bitcast.9, bf16[64,128]{1,0:T(8,128)(2,1)} %ow_hbm.1, ...), custom_call_target="tpu_custom_call" | custom-call | tf_op jit(solution)/shard_map/layer/pallas_call | solution.py:464
  68.0 0.7 copy.14

commit v5 on v4

--- a/solution.py
+++ b/solution.py
@@ -262,15 +262,15 @@
     first_start(DOWN)
     x_near(0)
     second_forward(ATTN, 0, 1)
+    first_rest(UP)
+    second_start(UP, 0)
     x_far(0)
     x_partner(0)
     norm_rows(xall, 0)
-    first_rest(UP)
-    second_start(UP, 0)
+    first_forward(DOWN)
+    second_start(UP, 1, 2, 3)
     second_rest(ATTN)
     x_start(1)
-    first_forward(DOWN)
-    second_start(UP, 1, 2, 3)
 
     weights = jnp.concatenate([attn[h, :, :, 0:128, :].reshape(D, 128) for h in range(2)], axis=1)
     qkvg[...] = jnp.dot(wide[...], weights, preferred_element_type=F32)
@@ -303,14 +303,15 @@
     for h in range(2):
         wo[tp, h] = attn[h, :, :, 128:160, :]
     x_forward(1)
+    second_forward(UP, 0)
     x_forward(2)
+    second_forward(UP, 1)
+    first_rest(DOWN)
+    second_start(DOWN, 0, 1, 2)
     x_near(2)
     x_near(1)
     x_far(2)
-    second_forward(UP, 0, 1)
     x_far(1)
-    first_rest(DOWN)
-    second_start(DOWN, 0, 1)
     x_partner(2)
     x_partner(1)
 
@@ -401,25 +402,26 @@
     swap(s0, 0)
     s1 = products(arrivals(0, False))
     swap(s1, 1)
-    deliver(s0, 0)
     second_forward(DOWN, 1)
-    second_start(DOWN, 2, 3)
+    second_start(DOWN, 3)
     s2 = products(arrivals(1, False))
     swap(s2, 2)
-    deliver(s1, 1)
-    deliver_on(0, s2, 2)
+    deliver_on(0, s0, 0)
+    deliver_on(0, s1, 1)
+    second_four(DOWN, 2, False)
+    s3 = products(arrivals(2, False))
+    swap(s3, 3)
+    deliver_on(1, s0, 0)
+    deliver_on(1, s1, 1)
+    deliver(s2, 2)
+    deliver_on(0, s3, 3)
     second_four(DOWN, 0, True)
-    s3 = products(arrivals(0, True))
-    swap(s3, 3)
-    deliver_on(1, s2, 2)
-    deliver_on(0, s3, 3)
-    second_four(DOWN, 1, True)
-    s4 = products(arrivals(1, True))
+    s4 = products(arrivals(0, True))
     swap(s4, 4)
     deliver_on(1, s3, 3)
     deliver_on(0, s4, 4)
-    second_four(DOWN, 2, False)
-    s5 = products(arrivals(2, False))
+    second_four(DOWN, 1, True)
+    s5 = products(arrivals(1, True))
     swap(s5, 5)
     deliver_on(1, s4, 4)
     deliver(s5, 5)

time: 68.7 us -> 68 us (0.990)
  Pallas kernels: 67.9 us -> 66.9 us
    pallas_call x1, Pallas kernels: 67.9 us -> 66.9 us  [local(): pl.pallas_call(layer_kernel, out_shape=pltpu.VMEM((ROWS, D // 8), BF), in...]
where the time goes in v5:
time: 68 us; the launch traced here: 67.6 us
  Pallas kernels  66.9 us (98%)
  local copies, waits for them, and re-layouts  0.68 us (1%)
    pallas_call x1, Pallas kernels, local(): pl.pallas_call(layer_kernel, out_shape=pltpu.VMEM((ROWS, D // 8), BF), in...  66.9 us

profile of v5, /device:TPU:2, one launch (start us, length us, event | category | flops | bytes accessed | tf_op | source)
XLA Modules:
  0.0 67.6 jit_solution(3755463344082775341)
XLA Ops:
  0.0 66.9 %layer.1 = bf16[384,256]{1,0:T(8,128)(2,1)S(1)} custom-call(bf16[384,256]{1,0:T(8,128)(2,1)} %act_hbm.1, f32[1,2048]{1,0:T(1,128)} %bitcast.10, bf16[64,128]{1,0:T(8,128)(2,1)} %bitcast.6, bf16[64,128]{1,0:T(8,128)(2,1)} %bitcast.7, bf16[64,128]{1,0:T(8,128)(2,1)} %bitcast.8, bf16[64,128]{1,0:T(8,128)(2,1)} %bitcast.9, bf16[64,128]{1,0:T(8,128)(2,1)} %ow_hbm.1, ...), custom_call_target="tpu_custom_call" | custom-call | tf_op jit(solution)/shard_map/layer/pallas_call | solution.py:466
  66.9 0.7 %copy.14 = bf16[384,256]{1,0:T(8,128)(2,1)} copy(bf16[384,256]{1,0:T(8,128)(2,1)S(1)} %layer.1) | data formatting | bytes 393216

commit v6 on v5

--- a/solution.py
+++ b/solution.py
@@ -70,8 +70,7 @@
     partner = {"tp": x * 2 + (1 - core)}
 
     barrier = pltpu.get_barrier_semaphore()
-    peers = [y_device(1), y_device(-1), z_device(1), z_device(-1), partner]
-    peers += [{"tp": x_index(step, c)} for step in (1, -1, 2) for c in range(2)]
+    peers = [y_device(1), y_device(-1), z_device(1), z_device(-1), x_device(1), x_device(-1), partner]
     for peer in peers:
         pl.semaphore_signal(barrier, inc=1, device_id=peer, device_id_type=MESH)
 
@@ -177,6 +176,11 @@
                     to = 1 - 2 * d
                     ref = second_block(item, half, -to, d, n)
                     send(ref, ref, ring_send.at[3 + item], second_sem(item, n, True), ring_device(half, 1, to))
+
+    def second_forward_on(c, item, n):
+        @pl.when(core == c)
+        def _():
+            second_forward(item, n)
 
     def second_rest(item):
         arrive(bufs[item].at[0], second_sem(item, 0, True))
@@ -307,7 +311,7 @@
     x_forward(2)
     second_forward(UP, 1)
     first_rest(DOWN)
-    second_start(DOWN, 0, 1, 2)
+    second_start(DOWN, 0, 1)
     x_near(2)
     x_near(1)
     x_far(2)
@@ -329,11 +333,12 @@
 
     norm_rows(mid, 1)
     second_rest(UP)
+    second_forward_on(1, DOWN, 0)
     for h in range(2):
         raw = jnp.dot(wide[...], upb[h].reshape(D, 512), preferred_element_type=F32)
         raw = jnp.maximum(raw, 0.0)
         hid[:, 512 * h : 512 * h + 512] = (raw * raw).astype(BF)
-    second_forward(DOWN, 0)
+    second_forward_on(0, DOWN, 0)
 
     def number(dz, dy):
         return (dz + 1) * 4 + dy + 1
@@ -403,25 +408,25 @@
     s1 = products(arrivals(0, False))
     swap(s1, 1)
     second_forward(DOWN, 1)
-    second_start(DOWN, 3)
+    second_start(DOWN, 2, 3)
     s2 = products(arrivals(1, False))
     swap(s2, 2)
     deliver_on(0, s0, 0)
     deliver_on(0, s1, 1)
-    second_four(DOWN, 2, False)
-    s3 = products(arrivals(2, False))
+    second_four(DOWN, 0, True)
+    s3 = products(arrivals(0, True))
     swap(s3, 3)
     deliver_on(1, s0, 0)
     deliver_on(1, s1, 1)
     deliver(s2, 2)
     deliver_on(0, s3, 3)
-    second_four(DOWN, 0, True)
-    s4 = products(arrivals(0, True))
+    second_four(DOWN, 1, True)
+    s4 = products(arrivals(1, True))
     swap(s4, 4)
     deliver_on(1, s3, 3)
     deliver_on(0, s4, 4)
-    second_four(DOWN, 1, True)
-    s5 = products(arrivals(1, True))
+    second_four(DOWN, 2, False)
+    s5 = products(arrivals(2, False))
     swap(s5, 5)
     deliver_on(1, s4, 4)
     deliver(s5, 5)

time: 68 us -> 66.5 us (0.978)
  Pallas kernels: 66.9 us -> 65.7 us
    pallas_call x1, Pallas kernels: 66.9 us -> 65.7 us  [local(): pl.pallas_call(layer_kernel, out_shape=pltpu.VMEM((ROWS, D // 8), BF), in...]
where the time goes in v6:
time: 66.5 us; the launch traced here: 66.4 us
  Pallas kernels  65.7 us (99%)
  local copies, waits for them, and re-layouts  0.68 us (1%)
    pallas_call x1, Pallas kernels, local(): pl.pallas_call(layer_kernel, out_shape=pltpu.VMEM((ROWS, D // 8), BF), in...  65.7 us

profile of v6, /device:TPU:2, one launch (start us, length us, event | category | flops | bytes accessed | tf_op | source)
XLA Modules:
  0.0 66.4 jit_solution(13098995406724110222)
XLA Ops:
  0.0 65.7 %layer.1 = bf16[384,256]{1,0:T(8,128)(2,1)S(1)} custom-call(bf16[384,256]{1,0:T(8,128)(2,1)} %act_hbm.1, f32[1,2048]{1,0:T(1,128)} %bitcast.10, bf16[64,128]{1,0:T(8,128)(2,1)} %bitcast.6, bf16[64,128]{1,0:T(8,128)(2,1)} %bitcast.7, bf16[64,128]{1,0:T(8,128)(2,1)} %bitcast.8, bf16[64,128]{1,0:T(8,128)(2,1)} %bitcast.9, bf16[64,128]{1,0:T(8,128)(2,1)} %ow_hbm.1, ...), custom_call_target="tpu_custom_call" | custom-call | tf_op jit(solution)/shard_map/layer/pallas_call | solution.py:471
  65.7 0.7 %copy.14 = bf16[384,256]{1,0:T(8,128)(2,1)} copy(bf16[384,256]{1,0:T(8,128)(2,1)S(1)} %layer.1) | data formatting | bytes 393216

commit v7 on v6

--- a/solution.py
+++ b/solution.py
@@ -17,7 +17,7 @@
 F32 = jnp.float32
 MESH = pl.DeviceIdType.MESH
 ATTN, UP, DOWN = 0, 1, 2
-ORDER = ((0, 1, 2, -1), (-1, 2, 0, 1))
+ORDER = ((0, 1, 2, -1), (2, -1, 0, 1))
 
 
 def rotary_tables():
@@ -47,7 +47,7 @@
     out_ref,
     attn, upb, dnb, xall, wo, ret, wide, mid, hid, pps, ppr, rss, rsr,
     small, gains, tables, qkvg, gat, lhs, acc,
-    local_sem, ring_send, first_recv, second_recv, x_send, x_recv, p_send, p_recv, r_send, r_recv,
+    hid2, ext, last, local_sem, ring_send, first_recv, second_recv, x_send, x_recv, p_send, p_recv, r_send, r_recv, h_send, h_recv,
 ):
     rep, fs, tp = lax.axis_index("rep"), lax.axis_index("fs"), lax.axis_index("tp")
     zl, y = lax.div(fs, 4), lax.rem(fs, 4)
@@ -339,9 +339,24 @@
         raw = jnp.maximum(raw, 0.0)
         hid[:, 512 * h : 512 * h + 512] = (raw * raw).astype(BF)
     second_forward_on(0, DOWN, 0)
+    send(hid, hid2, h_send.at[0], h_recv.at[0], partner)
 
     def number(dz, dy):
         return (dz + 1) * 4 + dy + 1
+
+    def last_start():
+        for half in range(2):
+            for d in range(2):
+                ref, sem = second_block(DOWN, half, 0, d, 3), second_sem(DOWN, 3, False)
+                there = ring_device(half, 1, 1 - 2 * d)
+
+                @pl.when(core == d)
+                def _():
+                    send(ref, ref, ring_send.at[3 + DOWN], sem, there)
+
+                @pl.when(core != d)
+                def _():
+                    send(ref, ext.at[half], ring_send.at[3 + DOWN], sem, {**there, "tp": x * 2 + d})
 
     begun = set()
 
@@ -370,26 +385,48 @@
             send(pps.at[n], ppr.at[n], p_send.at[0], p_recv.at[group], partner)
 
 
-    def route(at):
-        z_to, y_to = lax.rem(zl + at[0] + 4, 4), lax.rem(y + at[1] + 4, 4)
+    def route(dz, dy):
+        z_to, y_to = lax.rem(zl + dz + 4, 4), lax.rem(y + dy + 4, 4)
         c_to, k = lax.div(y_to, 2), lax.rem(y_to, 2)
         hops = lax.rem(z_to - x + 4, 4)
-        return number(*at), {"tp": z_to * 2 + c_to}, c_to, k, hops
+        return {"tp": z_to * 2 + c_to}, k, hops, (hops == 0) & (c_to == core), lax.div(3 - hops, 3) * (1 + k)
 
     def deliver(blocks, group):
         arrive(ppr.at[pl.ds(0, len(blocks))], p_recv.at[group])
         for at in blocks:
-            n, owner, c_to, k, hops = route(at)
+            n = number(*at)
+            owner, k, hops, own, sem = route(*at)
             total = (acc[n, rows_of(core), :] + ppr[n].astype(F32)).astype(BF)
             rss[n] = total
 
-            @pl.when((hops > 0) | (c_to != core))
+            @pl.when(jnp.logical_not(own))
             def _():
-                send(rss.at[n], rsr.at[hops, k, core], r_send.at[0], r_recv.at[0], owner)
-
-            @pl.when((hops == 0) & (c_to == core))
+                send(rss.at[n], rsr.at[hops, k, core], r_send.at[0], r_recv.at[sem], owner)
+
+            @pl.when(own)
             def _():
                 rsr[0, k, core] = total
+
+    step = 2 * core - 1
+
+    def deliver_last():
+        owner, k, hops, own, sem = route(step, step)
+        z_from, y_from = lax.rem(zl + step + 4, 4), lax.rem(y + step + 4, 4)
+        mine = jnp.concatenate([dnb[0, z_from, y_from], dnb[1, z_from, y_from]], axis=0)
+        other = ext[...].reshape(1024, 128)
+        for half in range(2):
+            rows = slice(192 * half, 192 * half + 192)
+            total = jnp.dot(hid[rows, :], mine, preferred_element_type=F32)
+            total = (total + jnp.dot(hid2[rows, :], other, preferred_element_type=F32)).astype(BF)
+            last[half] = total
+
+            @pl.when(jnp.logical_not(own))
+            def _():
+                send(last.at[half], rsr.at[hops, k, half], r_send.at[1], r_recv.at[sem], owner)
+
+            @pl.when(own)
+            def _():
+                rsr[0, k, half] = total
 
     def arrivals(n, far):
         step = (2, 2) if far else (-1, 1)
@@ -408,7 +445,8 @@
     s1 = products(arrivals(0, False))
     swap(s1, 1)
     second_forward(DOWN, 1)
-    second_start(DOWN, 2, 3)
+    second_start(DOWN, 2)
+    last_start()
     s2 = products(arrivals(1, False))
     swap(s2, 2)
     deliver_on(0, s0, 0)
@@ -430,13 +468,26 @@
     swap(s5, 5)
     deliver_on(1, s4, 4)
     deliver(s5, 5)
+    arrive(hid2, h_recv.at[0])
     second_four(DOWN, 3, False)
-    s6 = products(arrivals(3, False))
-    swap(s6, 6)
-    deliver(s6, 6)
+    deliver_last()
+
+    def late(k, c):
+        dz, dy = lax.rem(x - zl + 4, 4), lax.rem(core * 2 + k - y + 4, 4)
+        return (dz == (2 * c + 3) % 4) & (dy == (2 * c + 3) % 4)
 
     def collect():
-        arrive(rss.at[pl.ds(0, 14)], r_recv.at[0])
+        arrive(rss.at[pl.ds(0, 12)], r_recv.at[0])
+        for k in range(2):
+            first, second = late(k, 0), late(k, 1)
+
+            @pl.when((first & (core == 1)) | (second & (core == 0)))
+            def _():
+                arrive(rsr.at[0, k], r_recv.at[1 + k])
+
+            @pl.when(jnp.logical_not(first | second))
+            def _():
+                arrive(rsr.at[0, k, 1 - core], r_recv.at[1 + k])
 
     def finish():
         for k in range(2):
@@ -453,8 +504,12 @@
             sent(bufs[item].at[:, pl.ds(0, 3)], ring_send.at[3 + item])
         for which in range(3):
             sent(whole[which].at[pl.ds(0, 7)], x_send.at[which])
-        sent(pps, p_send.at[0])
-        sent(rss.at[pl.ds(0, 14)], r_send.at[0])
+        sent(hid, h_send.at[0])
+        sent(pps.at[pl.ds(0, 14)], p_send.at[0])
+        some = late(0, 0) | late(0, 1) | late(1, 0) | late(1, 1)
+        pl.when(some)(lambda: sent(rss.at[pl.ds(0, 13)], r_send.at[0]))
+        pl.when(jnp.logical_not(some))(lambda: sent(rss.at[pl.ds(0, 12)], r_send.at[0]))
+        pl.when(jnp.logical_not(route(step, step)[3]))(lambda: sent(last, r_send.at[1]))
 
     collect()
     finish()
@@ -494,7 +549,10 @@
             pltpu.VMEM((ROWS, 128), F32),
             pltpu.VMEM((ROWS, 512), BF),
             pltpu.VMEM((16, ROWS, 128), F32),
-            dma((7,)), dma((6,)), dma((6,)), dma((12,)), dma((3,)), dma((12,)), dma((1,)), dma((7,)), dma((1,)), dma((1,)),
+            pltpu.VMEM((ROWS, 1024), BF),
+            pltpu.VMEM((2, 512, 128), BF),
+            pltpu.VMEM((2, 192, 128), BF),
+            dma((7,)), dma((6,)), dma((6,)), dma((12,)), dma((3,)), dma((12,)), dma((1,)), dma((6,)), dma((2,)), dma((3,)), dma((1,)), dma((1,)),
         ],
         compiler_params=pltpu.CompilerParams(
             collective_id=0, has_side_effects=True, vmem_limit_bytes=56 * 1024 * 1024

time: 66.5 us -> 66.4 us (level)
  no operation moved by 1% of the time
where the time goes in v7:
time: 66.4 us; the launch traced here: 66.2 us
  Pallas kernels  65.6 us (99%)
  local copies, waits for them, and re-layouts  0.68 us (1%)
    pallas_call x1, Pallas kernels, local(): pl.pallas_call(layer_kernel, out_shape=pltpu.VMEM((ROWS, D // 8), BF), in...  65.6 us

profile of v7, /device:TPU:2, one launch (start us, length us, event | category | flops | bytes accessed | tf_op | source)
XLA Modules:
  0.0 66.2 jit_solution(15936706743239686403)
XLA Ops:
  0.0 65.6 %layer.1 = bf16[384,256]{1,0:T(8,128)(2,1)S(1)} custom-call(bf16[384,256]{1,0:T(8,128)(2,1)} %act_hbm.1, f32[1,2048]{1,0:T(1,128)} %bitcast.10, bf16[64,128]{1,0:T(8,128)(2,1)} %bitcast.6, bf16[64,128]{1,0:T(8,128)(2,1)} %bitcast.7, bf16[64,128]{1,0:T(8,128)(2,1)} %bitcast.8, bf16[64,128]{1,0:T(8,128)(2,1)} %bitcast.9, bf16[64,128]{1,0:T(8,128)(2,1)} %ow_hbm.1, ...), custom_call_target="tpu_custom_call" | custom-call | tf_op jit(solution)/shard_map/layer/pallas_call | solution.py:526
  65.6 0.7 %copy.14 = bf16[384,256]{1,0:T(8,128)(2,1)} copy(bf16[384,256]{1,0:T(8,128)(2,1)S(1)} %layer.1) | data formatting | bytes 393216

commit v8 on v7

--- a/solution.py
+++ b/solution.py
@@ -358,6 +358,9 @@
                 def _():
                     send(ref, ext.at[half], ring_send.at[3 + DOWN], sem, {**there, "tp": x * 2 + d})
 
+    def on_core(c, step):
+        pl.when(core == c)(step)
+
     begun = set()
 
     def products(pairs):
@@ -445,13 +448,14 @@
     s1 = products(arrivals(0, False))
     swap(s1, 1)
     second_forward(DOWN, 1)
-    second_start(DOWN, 2)
-    last_start()
+    on_core(0, lambda: second_start(DOWN, 2))
     s2 = products(arrivals(1, False))
     swap(s2, 2)
     deliver_on(0, s0, 0)
     deliver_on(0, s1, 1)
     second_four(DOWN, 0, True)
+    on_core(1, lambda: second_start(DOWN, 2))
+    on_core(0, last_start)
     s3 = products(arrivals(0, True))
     swap(s3, 3)
     deliver_on(1, s0, 0)
@@ -459,6 +463,7 @@
     deliver(s2, 2)
     deliver_on(0, s3, 3)
     second_four(DOWN, 1, True)
+    on_core(1, last_start)
     s4 = products(arrivals(1, True))
     swap(s4, 4)
     deliver_on(1, s3, 3)
@@ -467,10 +472,11 @@
     s5 = products(arrivals(2, False))
     swap(s5, 5)
     deliver_on(1, s4, 4)
-    deliver(s5, 5)
+    deliver_on(0, s5, 5)
     arrive(hid2, h_recv.at[0])
     second_four(DOWN, 3, False)
     deliver_last()
+    deliver_on(1, s5, 5)
 
     def late(k, c):
         dz, dy = lax.rem(x - zl + 4, 4), lax.rem(core * 2 + k - y + 4, 4)

time: 66.4 us -> 66.3 us (level)
  no operation moved by 1% of the time
where the time goes in v8:
time: 66.3 us; the launch traced here: 66.1 us
  Pallas kernels  65.5 us (99%)
  local copies, waits for them, and re-layouts  0.68 us (1%)
    pallas_call x1, Pallas kernels, local(): pl.pallas_call(layer_kernel, out_shape=pltpu.VMEM((ROWS, D // 8), BF), in...  65.5 us

profile of v8, /device:TPU:2, one launch (start us, length us, event | category | flops | bytes accessed | tf_op | source)
XLA Modules:
  0.0 66.1 jit_solution(2013578313822978380)
XLA Ops:
  0.0 65.5 %layer.1 = bf16[384,256]{1,0:T(8,128)(2,1)S(1)} custom-call(bf16[384,256]{1,0:T(8,128)(2,1)} %act_hbm.1, f32[1,2048]{1,0:T(1,128)} %bitcast.10, bf16[64,128]{1,0:T(8,128)(2,1)} %bitcast.6, bf16[64,128]{1,0:T(8,128)(2,1)} %bitcast.7, bf16[64,128]{1,0:T(8,128)(2,1)} %bitcast.8, bf16[64,128]{1,0:T(8,128)(2,1)} %bitcast.9, bf16[64,128]{1,0:T(8,128)(2,1)} %ow_hbm.1, ...), custom_call_target="tpu_custom_call" | custom-call | tf_op jit(solution)/shard_map/layer/pallas_call | solution.py:532
  65.5 0.7 %copy.14 = bf16[384,256]{1,0:T(8,128)(2,1)} copy(bf16[384,256]{1,0:T(8,128)(2,1)S(1)} %layer.1) | data formatting | bytes 393216

commit v9 on v8

--- a/solution.py
+++ b/solution.py
@@ -384,8 +384,16 @@
     def swap(blocks, group):
         for at in blocks:
             n = number(*at)
-            pps[n] = acc[n, rows_of(1 - core), :].astype(BF)
-            send(pps.at[n], ppr.at[n], p_send.at[0], p_recv.at[group], partner)
+            pps[n, 0] = acc[n, rows_of(1 - core), :].astype(BF)
+            send(pps.at[n, 0], ppr.at[n, 0], p_send.at[0], p_recv.at[group], partner)
+
+    def give(blocks, group):
+        @pl.when(core == 1)
+        def _():
+            for at in blocks:
+                n = number(*at)
+                pps[n] = acc[n].astype(BF).reshape(2, 192, 128)
+                send(pps.at[n], ppr.at[n], p_send.at[1], p_recv.at[group], partner)
 
 
     def route(dz, dy):
@@ -395,20 +403,38 @@
         return {"tp": z_to * 2 + c_to}, k, hops, (hops == 0) & (c_to == core), lax.div(3 - hops, 3) * (1 + k)
 
     def deliver(blocks, group):
-        arrive(ppr.at[pl.ds(0, len(blocks))], p_recv.at[group])
+        arrive(ppr.at[pl.ds(0, len(blocks)), 0], p_recv.at[group])
         for at in blocks:
             n = number(*at)
             owner, k, hops, own, sem = route(*at)
-            total = (acc[n, rows_of(core), :] + ppr[n].astype(F32)).astype(BF)
-            rss[n] = total
+            total = (acc[n, rows_of(core), :] + ppr[n, 0].astype(F32)).astype(BF)
+            rss[n, 0] = total
 
             @pl.when(jnp.logical_not(own))
             def _():
-                send(rss.at[n], rsr.at[hops, k, core], r_send.at[0], r_recv.at[sem], owner)
+                send(rss.at[n, 0], rsr.at[hops, k, core], r_send.at[0], r_recv.at[sem], owner)
 
             @pl.when(own)
             def _():
                 rsr[0, k, core] = total
+
+    def deliver_whole(blocks, group):
+        @pl.when(core == 0)
+        def _():
+            arrive(ppr.at[pl.ds(0, len(blocks))], p_recv.at[group])
+            for at in blocks:
+                n = number(*at)
+                owner, k, hops, own, sem = route(*at)
+                total = (acc[n].reshape(2, 192, 128) + ppr[n].astype(F32)).astype(BF)
+                rss[n] = total
+
+                @pl.when(jnp.logical_not(own))
+                def _():
+                    send(rss.at[n], rsr.at[hops, k], r_send.at[2], r_recv.at[sem], owner)
+
+                @pl.when(own)
+                def _():
+                    rsr[0, k] = total
 
     step = 2 * core - 1
 
@@ -457,43 +483,52 @@
     on_core(1, lambda: second_start(DOWN, 2))
     on_core(0, last_start)
     s3 = products(arrivals(0, True))
-    swap(s3, 3)
+    give(s3, 3)
     deliver_on(1, s0, 0)
     deliver_on(1, s1, 1)
     deliver(s2, 2)
-    deliver_on(0, s3, 3)
+    deliver_whole(s3, 3)
     second_four(DOWN, 1, True)
     on_core(1, last_start)
     s4 = products(arrivals(1, True))
-    swap(s4, 4)
-    deliver_on(1, s3, 3)
-    deliver_on(0, s4, 4)
+    give(s4, 4)
+    deliver_whole(s4, 4)
     second_four(DOWN, 2, False)
     s5 = products(arrivals(2, False))
-    swap(s5, 5)
-    deliver_on(1, s4, 4)
-    deliver_on(0, s5, 5)
+    give(s5, 5)
+    deliver_whole(s5, 5)
     arrive(hid2, h_recv.at[0])
     second_four(DOWN, 3, False)
     deliver_last()
-    deliver_on(1, s5, 5)
-
-    def late(k, c):
+
+    def among(k, blocks):
         dz, dy = lax.rem(x - zl + 4, 4), lax.rem(core * 2 + k - y + 4, 4)
-        return (dz == (2 * c + 3) % 4) & (dy == (2 * c + 3) % 4)
+        found = None
+        for at in blocks:
+            here = (dz == at[0] % 4) & (dy == at[1] % 4)
+            found = here if found is None else found | here
+        return found
+
+    halves = [among(k, s0 + s1 + s2) for k in range(2)]
+    on_one = [among(k, [(1, 1)]) for k in range(2)]
+    on_zero = [jnp.logical_not(halves[k] | on_one[k]) for k in range(2)]
+    whole_sums = [among(k, s3 + s4 + s5) for k in range(2)]
 
     def collect():
-        arrive(rss.at[pl.ds(0, 12)], r_recv.at[0])
+        arrive(rss.at[pl.ds(0, 6)], r_recv.at[0])
         for k in range(2):
-            first, second = late(k, 0), late(k, 1)
-
-            @pl.when((first & (core == 1)) | (second & (core == 0)))
+
+            @pl.when((on_zero[k] & (core == 1)) | (on_one[k] & (core == 0)))
             def _():
                 arrive(rsr.at[0, k], r_recv.at[1 + k])
 
-            @pl.when(jnp.logical_not(first | second))
+            @pl.when(halves[k])
             def _():
                 arrive(rsr.at[0, k, 1 - core], r_recv.at[1 + k])
+
+    def count(pair):
+        both, some = pair[0] & pair[1], pair[0] | pair[1]
+        return [jnp.logical_not(some), some & jnp.logical_not(both), both]
 
     def finish():
         for k in range(2):
@@ -511,10 +546,12 @@
         for which in range(3):
             sent(whole[which].at[pl.ds(0, 7)], x_send.at[which])
         sent(hid, h_send.at[0])
-        sent(pps.at[pl.ds(0, 14)], p_send.at[0])
-        some = late(0, 0) | late(0, 1) | late(1, 0) | late(1, 1)
-        pl.when(some)(lambda: sent(rss.at[pl.ds(0, 13)], r_send.at[0]))
-        pl.when(jnp.logical_not(some))(lambda: sent(rss.at[pl.ds(0, 12)], r_send.at[0]))
+        sent(pps.at[pl.ds(0, 5), 0], p_send.at[0])
+        pl.when(core == 1)(lambda: sent(pps.at[pl.ds(0, 9)], p_send.at[1]))
+        for own, here in enumerate(count(halves)):
+            pl.when(here)(lambda: sent(rss.at[pl.ds(0, 5 - own), 0], r_send.at[0]))
+        for own, here in enumerate(count(whole_sums)):
+            pl.when(here & (core == 0))(lambda: sent(rss.at[pl.ds(0, 9 - own)], r_send.at[2]))
         pl.when(jnp.logical_not(route(step, step)[3]))(lambda: sent(last, r_send.at[1]))
 
     collect()
@@ -544,9 +581,9 @@
             pltpu.VMEM((ROWS, D), BF),
             pltpu.VMEM((8, ROWS, 256), BF),
             pltpu.VMEM((ROWS, 1024), BF),
-            pltpu.VMEM((16, 192, 128), BF),
-            pltpu.VMEM((16, 192, 128), BF),
-            pltpu.VMEM((16, 192, 128), BF),
+            pltpu.VMEM((16, 2, 192, 128), BF),
+            pltpu.VMEM((16, 2, 192, 128), BF),
+            pltpu.VMEM((16, 2, 192, 128), BF),
             pltpu.VMEM((4, 2, 2, 192, 128), BF),
             pltpu.VMEM((4, 64, 128), BF),
             pltpu.VMEM((2, 1, D), F32),
@@ -558,7 +595,7 @@
             pltpu.VMEM((ROWS, 1024), BF),
             pltpu.VMEM((2, 512, 128), BF),
             pltpu.VMEM((2, 192, 128), BF),
-            dma((7,)), dma((6,)), dma((6,)), dma((12,)), dma((3,)), dma((12,)), dma((1,)), dma((6,)), dma((2,)), dma((3,)), dma((1,)), dma((1,)),
+            dma((7,)), dma((6,)), dma((6,)), dma((12,)), dma((3,)), dma((12,)), dma((2,)), dma((6,)), dma((3,)), dma((3,)), dma((1,)), dma((1,)),
         ],
         compiler_params=pltpu.CompilerParams(
             collective_id=0, has_side_effects=True, vmem_limit_bytes=56 * 1024 * 1024

time: 66.3 us -> 66.2 us (level)
  no operation moved by 1% of the time
where the time goes in v9:
time: 66.2 us; the launch traced here: 66.1 us
  Pallas kernels  65.4 us (99%)
  local copies, waits for them, and re-layouts  0.68 us (1%)
    pallas_call x1, Pallas kernels, local(): pl.pallas_call(layer_kernel, out_shape=pltpu.VMEM((ROWS, D // 8), BF), in...  65.4 us

profile of v9, /device:TPU:2, one launch (start us, length us, event | category | flops | bytes accessed | tf_op | source)
XLA Modules:
  0.0 66.1 jit_solution(17668187104244710637)
XLA Ops:
  0.0 65.4 %layer.1 = bf16[384,256]{1,0:T(8,128)(2,1)S(1)} custom-call(bf16[384,256]{1,0:T(8,128)(2,1)} %act_hbm.1, f32[1,2048]{1,0:T(1,128)} %bitcast.10, bf16[64,128]{1,0:T(8,128)(2,1)} %bitcast.6, bf16[64,128]{1,0:T(8,128)(2,1)} %bitcast.7, bf16[64,128]{1,0:T(8,128)(2,1)} %bitcast.8, bf16[64,128]{1,0:T(8,128)(2,1)} %bitcast.9, bf16[64,128]{1,0:T(8,128)(2,1)} %ow_hbm.1, ...), custom_call_target="tpu_custom_call" | custom-call | tf_op jit(solution)/shard_map/layer/pallas_call | solution.py:569
  65.4 0.7 %copy.14 = bf16[384,256]{1,0:T(8,128)(2,1)} copy(bf16[384,256]{1,0:T(8,128)(2,1)S(1)} %layer.1) | data formatting | bytes 393216

commit v10 on v9

--- a/solution.py
+++ b/solution.py
@@ -475,13 +475,13 @@
     swap(s1, 1)
     second_forward(DOWN, 1)
     on_core(0, lambda: second_start(DOWN, 2))
+    on_core(0, last_start)
     s2 = products(arrivals(1, False))
     swap(s2, 2)
     deliver_on(0, s0, 0)
     deliver_on(0, s1, 1)
     second_four(DOWN, 0, True)
     on_core(1, lambda: second_start(DOWN, 2))
-    on_core(0, last_start)
     s3 = products(arrivals(0, True))
     give(s3, 3)
     deliver_on(1, s0, 0)

time: 66.2 us -> 66.2 us (level)
  no operation moved by 1% of the time
where the time goes in v10:
time: 66.2 us; the launch traced here: 66.1 us
  Pallas kernels  65.4 us (99%)
  local copies, waits for them, and re-layouts  0.68 us (1%)
    pallas_call x1, Pallas kernels, local(): pl.pallas_call(layer_kernel, out_shape=pltpu.VMEM((ROWS, D // 8), BF), in...  65.4 us

profile of v10, /device:TPU:2, one launch (start us, length us, event | category | flops | bytes accessed | tf_op | source)
XLA Modules:
  0.0 66.1 jit_solution(7052582126594506822)
XLA Ops:
  0.0 65.4 %layer.1 = bf16[384,256]{1,0:T(8,128)(2,1)S(1)} custom-call(bf16[384,256]{1,0:T(8,128)(2,1)} %act_hbm.1, f32[1,2048]{1,0:T(1,128)} %bitcast.10, bf16[64,128]{1,0:T(8,128)(2,1)} %bitcast.6, bf16[64,128]{1,0:T(8,128)(2,1)} %bitcast.7, bf16[64,128]{1,0:T(8,128)(2,1)} %bitcast.8, bf16[64,128]{1,0:T(8,128)(2,1)} %bitcast.9, bf16[64,128]{1,0:T(8,128)(2,1)} %ow_hbm.1, ...), custom_call_target="tpu_custom_call" | custom-call | tf_op jit(solution)/shard_map/layer/pallas_call | solution.py:569
  65.4 0.7 %copy.14 = bf16[384,256]{1,0:T(8,128)(2,1)} copy(bf16[384,256]{1,0:T(8,128)(2,1)S(1)} %layer.1) | data formatting | bytes 393216
